TPU v7x, 32 devices: a whole 2x2x4 slice. The times are simulated.
32 devices in a mesh: rep: 2 (over x), fs: 8 (over z, y), tp: 2 (over core).
Axes of the slice: x: 2, y: 2, z: 4, core: 2. Of those that a mesh axis runs over, the one named last changes fastest.
Arguments:
- inputs: bfloat16 [4096, 2048], P(('rep', 'fs')), may hold values from -6 to 6
- cotangent: bfloat16 [4096, 2048], P(('rep', 'fs')), may hold values from -0.119628906 to 0.119628906
- up_weight: bfloat16 [2048, 4096], P('fs', 'tp'), may hold values from -0.125 to 0.125
- down_weight: bfloat16 [4096, 2048], P('tp', 'fs'), may hold values from -0.09375 to 0.09375
Outputs:
- grad_inputs: float32 [4096, 2048], P(('rep', 'fs'))
- grad_up: float32 [2048, 4096], P('fs', 'tp')
- grad_down: float32 [4096, 2048], P('tp', 'fs')
- norms_up: float32 [2048], P('fs')
- norms_down: float32 [4096], P('tp')
All inputs are finite; a program needn't handle non-finite values.
Results may differ from a plain program's by a relative error of at most 0.0029.
Values may be sent and summed in bfloat16 or wider, within the bound.
A program may use at most 128 MiB of HBM per device.

v0:
```python
import jax
import jax.numpy as jnp
from jax import lax
from jax.sharding import PartitionSpec as P

NARROW = jnp.bfloat16
CHUNKS = 2


def contract(left, right, left_dim, right_dim):
    return lax.dot_general(
        left, right, (((left_dim,), (right_dim,)), ((), ())), preferred_element_type=jnp.float32
    )


def own_block(blocks, axis, shift=0):
    size = lax.axis_size(axis)
    return lax.dynamic_index_in_dim(
        blocks, lax.rem(lax.axis_index(axis) + shift, size), 0, keepdims=False
    )


def rotate(block, axis, shift):
    size = lax.axis_size(axis)
    return lax.ppermute(block, axis, [(at, (at + shift) % size) for at in range(size)])


def scatter_sum(blocks, axis):
    total = own_block(blocks, axis)
    for shift in range(1, lax.axis_size(axis)):
        sent = own_block(blocks, axis, shift).astype(NARROW)
        total = total + rotate(sent, axis, shift).astype(jnp.float32)
    return total


def gather_blocks(block, axis):
    size = lax.axis_size(axis)
    me = lax.axis_index(axis)
    held = [block] + [rotate(block, axis, shift) for shift in range(1, size)]
    placed = []
    for at in range(size):
        pick = held[0]
        for shift in range(1, size):
            pick = jnp.where(lax.rem(me - at + size, size) == shift, held[shift], pick)
        placed.append(pick)
    return jnp.stack(placed)


def fs_sum(blocks, ahead=None):
    groups = lax.axis_size("fs")
    pair = 2 if groups % 2 == 0 else 1
    far = groups // pair
    me = lax.axis_index("fs")
    blocks = blocks.reshape((far, pair) + blocks.shape[1:])

    def near_block(shift):
        return lax.dynamic_index_in_dim(
            blocks, lax.rem(lax.rem(me, pair) + shift, pair), 1, keepdims=False
        )

    held = near_block(0)
    for shift in range(1, pair):
        perm = [(at, at - at % pair + (at + shift) % pair) for at in range(groups)]
        got = lax.ppermute(near_block(shift).astype(NARROW), "fs", perm)
        held = held + got.astype(jnp.float32)

    if ahead is not None:
        held, ahead = lax.optimization_barrier((held, ahead))

    def far_block(shift):
        return lax.dynamic_index_in_dim(held, lax.rem(me // pair + shift, far), 0, keepdims=False)

    total = far_block(0)
    for shift in range(1, far):
        perm = [(at, (at + shift * pair) % groups) for at in range(groups)]
        got = lax.ppermute(far_block(shift).astype(NARROW), "fs", perm)
        total = total + got.astype(jnp.float32)
    return total, ahead


def exchange(blocks, axis):
    return lax.all_to_all(blocks, axis, 0, 0)


def small_sum(value, axis):
    size = lax.axis_size(axis)
    if size & (size - 1):
        return lax.psum(value, axis)
    bit = 1
    while bit < size:
        value = value + lax.ppermute(value, axis, [(at, at ^ bit) for at in range(size)])
        bit *= 2
    return value


def token_plan(inputs, cotangent, up_weight, down_weight):
    reps, groups, cores = (lax.axis_size(axis) for axis in ("rep", "fs", "tp"))
    rows, width = inputs.shape
    depth, units = up_weight.shape
    mine = units // groups
    part = depth // reps
    half = width // cores

    few = mine // reps
    up = own_block(up_weight.reshape(reps, part, groups, mine).transpose(0, 2, 1, 3), "rep")
    down = own_block(down_weight.reshape(groups, reps, few, depth).transpose(1, 0, 2, 3), "rep")
    both = jnp.concatenate([up, down.reshape(groups, part, mine)], axis=1)
    both = gather_blocks(exchange(both, "fs"), "rep")
    up = both[:, :, :part].transpose(1, 0, 2, 3).reshape(width, mine)
    down = both[:, :, part:].reshape(reps, groups, few, depth)
    down = down.transpose(0, 2, 1, 3).reshape(mine, width)
    tokens = lax.all_gather(
        own_block(inputs.reshape(cores, rows // cores, width), "tp"), ("fs", "tp"), axis=0, tiled=True
    )
    cot = lax.all_gather(
        own_block(cotangent.reshape(cores, rows // cores, width), "tp"), ("fs", "tp"), axis=0, tiled=True
    )

    pre_act = contract(tokens, up, 1, 0)
    act_grad = contract(cot, down, 1, 1)
    rectified = jnp.maximum(pre_act, 0.0)
    hidden = (rectified * rectified).astype(jnp.bfloat16)
    pre_grad = (2.0 * rectified * act_grad).astype(jnp.bfloat16)

    up_rows = up.reshape(cores, half, mine)
    share = contract(pre_grad, own_block(up_rows, "tp"), 1, 1)
    for shift in range(1, cores):
        sent = contract(pre_grad, own_block(up_rows, "tp", shift), 1, 1).astype(NARROW)
        share = share + rotate(sent, "tp", shift).astype(jnp.float32)
    chunks = CHUNKS if half % (128 * CHUNKS) == 0 else 1
    share = share.reshape(groups, rows, half)
    step = half // chunks
    def spread(term):
        term = term.reshape(groups, reps, part, mine).transpose(1, 0, 2, 3)
        return exchange(scatter_sum(term, "rep").astype(NARROW), "fs")

    def whole(term):
        term = gather_blocks(term, "rep")
        return term.transpose(0, 2, 1, 3).reshape(depth, units).astype(jnp.float32)

    spreads = (spread(contract(cot, hidden, 0, 0)), spread(contract(tokens, pre_grad, 0, 0)))
    sums = []
    for at in range(chunks):
        ahead = spreads if at == chunks - 1 else None
        total, ahead = fs_sum(share[:, :, at * step : (at + 1) * step], ahead)
        sums.append(total)
    share = jnp.concatenate(sums, axis=1)
    share = gather_blocks(share, "tp")
    grad_inputs = share.transpose(1, 0, 2).reshape(rows, width)

    down_turned, grad_up = whole(ahead[0]), whole(ahead[1])
    norms_up = small_sum(jnp.sum(grad_up * grad_up, axis=1), "tp")
    norms_down = small_sum(jnp.sum(down_turned * down_turned, axis=0), "fs")
    return (grad_inputs, grad_up, down_turned.T, norms_up, norms_down)


def weight_plan(inputs, cotangent, up_weight, down_weight):
    up_whole = lax.all_gather(up_weight, "fs", axis=0, tiled=True)
    pre_act = jnp.dot(inputs, up_whole, preferred_element_type=jnp.float32)
    act_grad = contract(cotangent, lax.all_gather(down_weight, "fs", axis=1, tiled=True), 1, 1)
    rectified = jnp.maximum(pre_act, 0.0)
    hidden = (rectified * rectified).astype(jnp.bfloat16)
    pre_grad = (2.0 * rectified * act_grad).astype(jnp.bfloat16)
    up_part = lax.psum_scatter(
        contract(inputs, pre_grad, 0, 0), "fs", scatter_dimension=0, tiled=True
    )
    down_part = lax.psum_scatter(
        contract(cotangent, hidden, 0, 0), "fs", scatter_dimension=0, tiled=True
    )
    grad_up, down_turned = lax.psum((up_part, down_part), "rep")
    grad_inputs = lax.psum(contract(pre_grad, up_whole, 1, 1), "tp")
    norms_up = lax.psum(jnp.sum(grad_up * grad_up, axis=1), "tp")
    norms_down = lax.psum(jnp.sum(down_turned * down_turned, axis=0), "fs")
    grad_down = down_turned.T
    return (grad_inputs, grad_up, grad_down, norms_up, norms_down)


def shards(inputs, cotangent, up_weight, down_weight):
    tokens = inputs.size * lax.axis_size("fs") // lax.axis_size("tp")
    weights = up_weight.size * lax.axis_size("fs")
    plan = token_plan if tokens <= weights else weight_plan
    return plan(inputs, cotangent, up_weight, down_weight)


def solution(mesh):
    return jax.shard_map(
        shards,
        mesh=mesh,
        in_specs=(P(("rep", "fs"), None), P(("rep", "fs"), None), P("fs", "tp"), P("tp", "fs")),
        out_specs=(P(("rep", "fs"), None), P("fs", "tp"), P("tp", "fs"), P("fs"), P("tp")),
        check_vma=False,
    )
```

profile of v0, /device:TPU:0, one launch (start us, length us, event | category | flops | bytes accessed | tf_op | source)
XLA Modules:
  0.0 341.9 jit_solution(2736152882394223812)
XLA Ops:
  7.2 1.1 copy-done
  8.4 0.8 constant_dynamic-slice_fusion.1
  9.3 2.0 constant_dynamic-slice_fusion
  12.4 49.7 %all_to_all.15 = bf16[8,256,256]{2,1,0:T(8,128)(2,1)S(1)} all-to-all(bf16[8,256,256]{2,1,0:T(8,128)(2,1)S(1)} %copy.33), channel_id=1, replica_groups=mesh['rep'=2,'fs'=8,'tp'=2] {'fs'}, dimensions={0} | all-to-all | bytes 2097152 | tf_op jit(solution)/shard_map/all_to_all | solution.py:82
  62.1 1.5 collective-permute-start
  63.6 22.0 %collective-permute-done = bf16[8,256,256]{2,1,0:T(8,128)(2,1)S(1)} collective-permute-done((bf16[8,256,256]{2,1,0:T(8,128)(2,1)S(1)}, bf16[8,256,256]{2,1,0:T(8,128)(2,1)S(1)}, u32[]{:S(2)}, u32[]{:S(2)}) %collective-permute-start) | collective-permute-done | bytes 1048608 | tf_op jit(solution)/shard_map/ppermute | solution.py:25
  85.9 0.6 copy.35
  86.8 18.6 %all-gather.5.cloned.1.call-done = bf16[1,2048,2048]{2,1,0:T(8,128)(2,1)} async-done(((bf16[1,128,2048]{2,1,0:T(8,128)(2,1)}), bf16[1,2048,2048]{2,1,0:T(8,128)(2,1)}) %all-gather.5.cloned.1.call-update) | async-done | bytes 8388624 | tf_op jit(solution)/shard_map/all_gather | solution.py:112
  105.4 7.1 %fusion.8 = f32[2048,256]{1,0:T(8,128)} fusion(bf16[2048,256]{1,0:T(8,128)(2,1)S(1)} %bitcast.161, bf16[1,2048,2048]{2,1,0:T(8,128)(2,1)} %all-gather.5.cloned.1.call-done), kind=kOutput, calls=%fused_computation.10 | convolution fusion | flops 2148007936 | bytes 11534336 | tf_op jit(solution)/shard_map/dot_general | solution.py:11
  112.5 68.6 %all-gather.7.cloned.1.call-done = bf16[1,2048,2048]{2,1,0:T(8,128)(2,1)} async-done(((bf16[1,128,2048]{2,1,0:T(8,128)(2,1)}), bf16[1,2048,2048]{2,1,0:T(8,128)(2,1)}) %all-gather.7.cloned.1.call-update) | async-done | bytes 8388624 | tf_op jit(solution)/shard_map/all_gather | solution.py:115
  181.0 6.4 %fusion.14 = bf16[2048,256]{1,0:T(8,128)(2,1)S(1)} fusion(bf16[256,2048]{1,0:T(8,128)(2,1)S(1)} %bitcast.174, bf16[1,2048,2048]{2,1,0:T(8,128)(2,1)} %all-gather.7.cloned.1.call-done, f32[2048,256]{1,0:T(8,128)} %fusion.8), kind=kOutput, calls=%fused_computation.16 | convolution fusion | flops 2149056512 | bytes 12582912 | tf_op jit(solution)/shard_map/dot_general | solution.py:11
  187.4 3.3 convolution_convert_fusion
  191.0 6.1 %fusion.4 = f32[2048,256]{1,0:T(8,128)S(1)} fusion(bf16[2048,256]{1,0:T(8,128)(2,1)S(1)} %fusion.14, bf16[1,2048,2048]{2,1,0:T(8,128)(2,1)} %all-gather.5.cloned.1.call-done), kind=kOutput, calls=%fused_computation.4 | convolution fusion | flops 2147483648 | bytes 11534336 | tf_op jit(solution)/shard_map/dot_general | solution.py:11
  197.2 1.5 collective-permute-start.8
  198.7 7.4 %fusion = f32[2048,256]{1,0:T(8,128)} fusion(bf16[1,2048,2048]{2,1,0:T(8,128)(2,1)} %all-gather.7.cloned.1.call-done, f32[2048,256]{1,0:T(8,128)S(1)} %copy-done.10), kind=kOutput, calls=%fused_computation | convolution fusion | flops 2148532224 | bytes 12582912 | tf_op jit(solution)/shard_map/dot_general | solution.py:11
  206.1 5.2 %collective-permute-done.8 = bf16[8,128,256]{2,1,0:T(8,128)(2,1)S(1)} collective-permute-done((bf16[8,128,256]{2,1,0:T(8,128)(2,1)S(1)}, bf16[8,128,256]{2,1,0:T(8,128)(2,1)S(1)}, u32[]{:S(2)}, u32[]{:S(2)}) %collective-permute-start.8) | collective-permute-done | bytes 524320 | tf_op jit(solution)/shard_map/ppermute | solution.py:25
  211.3 0.9 fusion.23
  212.3 4.1 %all-to-all-start.2 = ((bf16[8,128,256]{2,1,0:T(8,128)(2,1)}), bf16[8,128,256]{2,1,0:T(8,128)(2,1)}, u32[]{:S(2)}, u32[]{:S(2)}) async-start(bf16[8,128,256]{2,1,0:T(8,128)(2,1)} %fusion.23), calls=%async_computation.2 | async-start | bytes 1048576 | tf_op jit(solution)/shard_map/all_to_all | solution.py:82
  216.4 3.5 %convert_add_fusion = f32[2048,1024]{1,0:T(8,128)S(1)} fusion(bf16[2048,1024]{1,0:T(8,128)(2,1)} %collective-permute-done.1, bf16[2048,256]{1,0:T(8,128)(2,1)S(1)} %fusion.14, bf16[2,1024,256]{2,1,0:T(8,128)(2,1)S(1)} %bitcast.163, s32[]{:T(128)S(6)} %select_n.111), kind=kOutput, calls=%fused_computation.8 | convolution fusion | flops 1077936128 | bytes 14155780 | tf_op jit(solution)/shard_map/dot_general | solution.py:11
  219.9 1.4 fusion.46
  221.5 1.9 collective-permute-start.2
  223.5 1.1 copy-done.7
  224.6 1.5 collective-permute-start.7
  226.3 1.9 collective-permute-start.6
  228.2 9.7 %collective-permute-done.7 = bf16[8,128,256]{2,1,0:T(8,128)(2,1)S(1)} collective-permute-done((bf16[8,128,256]{2,1,0:T(8,128)(2,1)S(1)}, bf16[8,128,256]{2,1,0:T(8,128)(2,1)S(1)}, u32[]{:S(2)}, u32[]{:S(2)}) %collective-permute-start.7) | collective-permute-done | bytes 524320 | tf_op jit(solution)/shard_map/ppermute | solution.py:25
  237.9 0.9 fusion.24
  238.9 5.6 %all-to-all-start.1 = ((bf16[8,128,256]{2,1,0:T(8,128)(2,1)}), bf16[8,128,256]{2,1,0:T(8,128)(2,1)}, u32[]{:S(2)}, u32[]{:S(2)}) async-start(bf16[8,128,256]{2,1,0:T(8,128)(2,1)} %fusion.24), calls=%async_computation.1 | async-start | bytes 1048576 | tf_op jit(solution)/shard_map/all_to_all | solution.py:82
  244.5 6.3 %collective-permute-done.2 = bf16[4,256,512]{2,1,0:T(8,128)(2,1)S(1)} collective-permute-done((bf16[4,256,512]{2,1,0:T(8,128)(2,1)S(1)}, bf16[4,256,512]{2,1,0:T(8,128)(2,1)S(1)}, u32[]{:S(2)}, u32[]{:S(2)}) %collective-permute-start.2) | collective-permute-done | bytes 1048608 | tf_op jit(solution)/shard_map/ppermute | solution.py:64
  250.7 2.1 bitcast_add_fusion.1
  252.8 1.0 fusion.38
  253.9 3.0 collective-permute-start.3
  256.9 1.1 collective-permute-start.5
  257.9 1.8 collective-permute-start.4
  259.8 15.8 %collective-permute-done.6 = bf16[4,256,512]{2,1,0:T(8,128)(2,1)} collective-permute-done((bf16[4,256,512]{2,1,0:T(8,128)(2,1)S(1)}, bf16[4,256,512]{2,1,0:T(8,128)(2,1)}, u32[]{:S(2)}, u32[]{:S(2)}) %collective-permute-start.6) | collective-permute-done | bytes 1048608 | tf_op jit(solution)/shard_map/ppermute | solution.py:64
  275.6 1.5 bitcast_add_fusion
  277.1 0.8 fusion.41
  277.9 1.7 collective-permute-start.9
  279.6 2.1 collective-permute-start.11
  281.8 0.8 collective-permute-start.10
  282.6 1.5 collective-permute-start.13
  284.6 1.4 fusion.30
  286.1 3.2 collective-permute-done.9
  289.2 2.9 collective-permute-done.11
  292.2 11.5 %collective-permute-done.10 = bf16[256,512]{1,0:T(8,128)(2,1)} collective-permute-done((bf16[256,512]{1,0:T(8,128)(2,1)S(1)}, bf16[256,512]{1,0:T(8,128)(2,1)}, u32[]{:S(2)}, u32[]{:S(2)}) %collective-permute-start.10) | collective-permute-done | bytes 262176 | tf_op jit(solution)/shard_map/ppermute | solution.py:76
  303.7 1.2 fusion.28
  304.9 1.1 pad_maximum_fusion.3
  306.0 1.1 select_bitcast_fusion.4
  307.8 1.1 select_bitcast_fusion.6
  309.6 1.5 collective-permute-done.16
  311.1 1.0 collective-permute-start.17
  312.2 1.5 convert_bitcast_fusion.1
  313.6 2.3 copy.41
  315.9 3.2 copy.52
  319.1 1.2 copy.40
  320.4 2.2 copy.48
  322.6 0.6 collective-permute-start.18
  323.2 0.6 bitcast_add_fusion.6
  323.7 3.4 collective-permute-done.18
  327.1 0.6 add.167
  327.7 1.4 select_bitcast_fusion
  329.1 1.1 copy.39
  330.2 0.7 stack.40
  330.9 1.9 pad_maximum_fusion
  332.8 2.2 copy.47
  (59 shorter events, 4.3 us)
Async XLA Ops:
  7.2 1.2 copy-start
  7.2 4.1 %copy-start.9 = (bf16[2048,256]{1,0:T(8,128)(2,1)S(1)}, bf16[2048,256]{1,0:T(8,128)(2,1)}, u32[]{:S(2)}) copy-start(bf16[2048,256]{1,0:T(8,128)(2,1)} %param.7) | copy-start | bytes 3145732
  7.2 98.2 %all-gather.5.cloned.1.call-start = ((), (), s32[]{:S(2)}) async-start(), calls=%async_computation.3 | async-start | bytes 8912896 | tf_op jit(solution)/shard_map/all_gather | solution.py:112
  9.2 2.4 copy-start.8
  9.3 171.8 %all-gather.7.cloned.1.call-start = ((), (), s32[]{:S(2)}) async-start(), calls=%async_computation.4 | async-start | bytes 8912896 | tf_op jit(solution)/shard_map/all_gather | solution.py:115
  62.1 23.5 %collective-permute-start = (bf16[8,256,256]{2,1,0:T(8,128)(2,1)S(1)}, bf16[8,256,256]{2,1,0:T(8,128)(2,1)S(1)}, u32[]{:S(2)}, u32[]{:S(2)}) collective-permute-start(bf16[8,256,256]{2,1,0:T(8,128)(2,1)S(1)} %all_to_all.15), channel_id=1, source_target_pairs={{0,16},{16,0},{1,17},{17,1},{2,18},{18,2},{3,19},{19,3},{4,20},{20... | collective-permute-start | bytes 3145736 | tf_op jit(solution)/shard_map/ppermute | solution.py:25
  190.7 25.7 %collective-permute-start.1 = (bf16[2048,1024]{1,0:T(8,128)(2,1)}, bf16[2048,1024]{1,0:T(8,128)(2,1)}, u32[]{:S(2)}, u32[]{:S(2)}) collective-permute-start(bf16[2048,1024]{1,0:T(8,128)(2,1)} %convolution_convert_fusion), channel_id=1, source_target_pairs={{0,1},{1,0},{2,3},{3,2},{4,5},{5,4},{6,7},{7,6},{8,9},{9,8},{10,11... | collective-permute-start | bytes 12582920 | tf_op jit(solution)/shard_map/ppermute | solution.py:25
  191.0 7.7 %copy-start.10 = (f32[2048,256]{1,0:T(8,128)S(1)}, f32[2048,256]{1,0:T(8,128)}, u32[]{:S(2)}) copy-start(f32[2048,256]{1,0:T(8,128)} %fusion.8) | copy-start | bytes 6291460
  197.2 14.2 %collective-permute-start.8 = (bf16[8,128,256]{2,1,0:T(8,128)(2,1)S(1)}, bf16[8,128,256]{2,1,0:T(8,128)(2,1)S(1)}, u32[]{:S(2)}, u32[]{:S(2)}) collective-permute-start(bf16[8,128,256]{2,1,0:T(8,128)(2,1)S(1)} %fusion.26), channel_id=1, source_target_pairs={{0,16},{16,0},{1,17},{17,1},{2,18},{18,2},{3,19},{19,3},{4,20},{20... | collective-permute-start | bytes 1572872 | tf_op jit(solution)/shard_map/ppermute | solution.py:25
  212.3 26.6 %all-to-all-start.2 = ((bf16[8,128,256]{2,1,0:T(8,128)(2,1)}), bf16[8,128,256]{2,1,0:T(8,128)(2,1)}, u32[]{:S(2)}, u32[]{:S(2)}) async-start(bf16[8,128,256]{2,1,0:T(8,128)(2,1)} %fusion.23), calls=%async_computation.2 | async-start | bytes 1048576 | tf_op jit(solution)/shard_map/all_to_all | solution.py:82
  221.4 4.9 %copy-start.2 = (f32[8,256,512]{2,1,0:T(8,128)}, f32[8,256,512]{2,1,0:T(8,128)S(1)}, u32[]{:S(2)}) copy-start(f32[8,256,512]{2,1,0:T(8,128)S(1)} %get-tuple-element.12) | copy-start | bytes 12582916
  221.4 6.9 %copy-start.4 = (f32[8,256,512]{2,1,0:T(8,128)}, f32[8,256,512]{2,1,0:T(8,128)S(1)}, u32[]{:S(2)}) copy-start(f32[8,256,512]{2,1,0:T(8,128)S(1)} %get-tuple-element.11) | copy-start | bytes 12582916
  221.4 3.2 copy-start.7
  221.5 29.2 %collective-permute-start.2 = (bf16[4,256,512]{2,1,0:T(8,128)(2,1)S(1)}, bf16[4,256,512]{2,1,0:T(8,128)(2,1)S(1)}, u32[]{:S(2)}, u32[]{:S(2)}) collective-permute-start(bf16[4,256,512]{2,1,0:T(8,128)(2,1)S(1)} %fusion.19), channel_id=1, source_target_pairs={{0,2},{2,0},{4,6},{6,4},{8,10},{10,8},{12,14},{14,12},{1,3},{3,1},... | collective-permute-start | bytes 3145736 | tf_op jit(solution)/shard_map/ppermute | solution.py:64
  224.6 13.3 %collective-permute-start.7 = (bf16[8,128,256]{2,1,0:T(8,128)(2,1)S(1)}, bf16[8,128,256]{2,1,0:T(8,128)(2,1)S(1)}, u32[]{:S(2)}, u32[]{:S(2)}) collective-permute-start(bf16[8,128,256]{2,1,0:T(8,128)(2,1)S(1)} %fusion.25), channel_id=1, source_target_pairs={{0,16},{16,0},{1,17},{17,1},{2,18},{18,2},{3,19},{19,3},{4,20},{20... | collective-permute-start | bytes 1572872 | tf_op jit(solution)/shard_map/ppermute | solution.py:25
  226.3 49.2 %collective-permute-start.6 = (bf16[4,256,512]{2,1,0:T(8,128)(2,1)S(1)}, bf16[4,256,512]{2,1,0:T(8,128)(2,1)}, u32[]{:S(2)}, u32[]{:S(2)}) collective-permute-start(bf16[4,256,512]{2,1,0:T(8,128)(2,1)S(1)} %fusion.20), channel_id=1, source_target_pairs={{0,2},{2,0},{4,6},{6,4},{8,10},{10,8},{12,14},{14,12},{1,3},{3,1},... | collective-permute-start | bytes 3145736 | tf_op jit(solution)/shard_map/ppermute | solution.py:64
  238.9 38.2 %all-to-all-start.1 = ((bf16[8,128,256]{2,1,0:T(8,128)(2,1)}), bf16[8,128,256]{2,1,0:T(8,128)(2,1)}, u32[]{:S(2)}, u32[]{:S(2)}) async-start(bf16[8,128,256]{2,1,0:T(8,128)(2,1)} %fusion.24), calls=%async_computation.1 | async-start | bytes 1048576 | tf_op jit(solution)/shard_map/all_to_all | solution.py:82
  250.7 24.8 %copy-start.3 = (f32[8,256,512]{2,1,0:T(8,128)S(1)}, f32[8,256,512]{2,1,0:T(8,128)}, u32[]{:S(2)}) copy-start(f32[8,256,512]{2,1,0:T(8,128)} %copy-done.2) | copy-start | bytes 12582916
  252.8 6.9 %copy-start.6 = (f32[4,256,512]{2,1,0:T(8,128)}, f32[4,256,512]{2,1,0:T(8,128)S(1)}, u32[]{:S(2)}) copy-start(f32[4,256,512]{2,1,0:T(8,128)S(1)} %bitcast_add_fusion.1) | copy-start | bytes 6291460
  253.9 27.9 %collective-permute-start.3 = (bf16[256,512]{1,0:T(8,128)(2,1)}, bf16[256,512]{1,0:T(8,128)(2,1)}, u32[]{:S(2)}, u32[]{:S(2)}) collective-permute-start(bf16[256,512]{1,0:T(8,128)(2,1)} %get-tuple-element.15), channel_id=1, source_target_pairs={{0,4},{2,6},{4,8},{6,10},{8,12},{10,14},{12,0},{14,2},{1,5},{3,7},... | collective-permute-start | bytes 786440 | tf_op jit(solution)/shard_map/ppermute | solution.py:76
  256.9 25.7 %collective-permute-start.5 = (bf16[256,512]{1,0:T(8,128)(2,1)}, bf16[256,512]{1,0:T(8,128)(2,1)}, u32[]{:S(2)}, u32[]{:S(2)}) collective-permute-start(bf16[256,512]{1,0:T(8,128)(2,1)} %get-tuple-element.16), channel_id=1, source_target_pairs={{0,12},{2,14},{4,0},{6,2},{8,4},{10,6},{12,8},{14,10},{1,13},{3,15... | collective-permute-start | bytes 786440 | tf_op jit(solution)/shard_map/ppermute | solution.py:76
  257.9 26.1 %collective-permute-start.4 = (bf16[256,512]{1,0:T(8,128)(2,1)S(1)}, bf16[256,512]{1,0:T(8,128)(2,1)}, u32[]{:S(2)}, u32[]{:S(2)}) collective-permute-start(bf16[256,512]{1,0:T(8,128)(2,1)S(1)} %get-tuple-element.17), channel_id=1, source_target_pairs={{0,8},{2,10},{4,12},{6,14},{8,0},{10,2},{12,4},{14,6},{1,9},{3,11}... | collective-permute-start | bytes 786440 | tf_op jit(solution)/shard_map/ppermute | solution.py:76
  277.9 11.3 %collective-permute-start.9 = (bf16[256,512]{1,0:T(8,128)(2,1)}, bf16[256,512]{1,0:T(8,128)(2,1)}, u32[]{:S(2)}, u32[]{:S(2)}) collective-permute-start(bf16[256,512]{1,0:T(8,128)(2,1)} %get-tuple-element.18), channel_id=1, source_target_pairs={{0,4},{2,6},{4,8},{6,10},{8,12},{10,14},{12,0},{14,2},{1,5},{3,7},... | collective-permute-start | bytes 786440 | tf_op jit(solution)/shard_map/ppermute | solution.py:76
  279.6 12.6 %collective-permute-start.11 = (bf16[256,512]{1,0:T(8,128)(2,1)S(1)}, bf16[256,512]{1,0:T(8,128)(2,1)}, u32[]{:S(2)}, u32[]{:S(2)}) collective-permute-start(bf16[256,512]{1,0:T(8,128)(2,1)S(1)} %get-tuple-element.19), channel_id=1, source_target_pairs={{0,12},{2,14},{4,0},{6,2},{8,4},{10,6},{12,8},{14,10},{1,13},{3,15... | collective-permute-start | bytes 786440 | tf_op jit(solution)/shard_map/ppermute | solution.py:76
  281.8 21.9 %collective-permute-start.10 = (bf16[256,512]{1,0:T(8,128)(2,1)S(1)}, bf16[256,512]{1,0:T(8,128)(2,1)}, u32[]{:S(2)}, u32[]{:S(2)}) collective-permute-start(bf16[256,512]{1,0:T(8,128)(2,1)S(1)} %get-tuple-element.20), channel_id=1, source_target_pairs={{0,8},{2,10},{4,12},{6,14},{8,0},{10,2},{12,4},{14,6},{1,9},{3,11}... | collective-permute-start | bytes 786440 | tf_op jit(solution)/shard_map/ppermute | solution.py:76
  282.6 25.2 %collective-permute-start.13 = (bf16[8,128,256]{2,1,0:T(8,128)(2,1)}, bf16[8,128,256]{2,1,0:T(8,128)(2,1)S(1)}, u32[]{:S(2)}, u32[]{:S(2)}) collective-permute-start(bf16[8,128,256]{2,1,0:T(8,128)(2,1)} %all-to-all-done.2), channel_id=1, source_target_pairs={{0,16},{16,0},{1,17},{17,1},{2,18},{18,2},{3,19},{19,3},{4,20},{20... | collective-permute-start | bytes 1572872 | tf_op jit(solution)/shard_map/ppermute | solution.py:25
  284.1 22.0 %collective-permute-start.14 = (bf16[8,128,256]{2,1,0:T(8,128)(2,1)}, bf16[8,128,256]{2,1,0:T(8,128)(2,1)S(1)}, u32[]{:S(2)}, u32[]{:S(2)}) collective-permute-start(bf16[8,128,256]{2,1,0:T(8,128)(2,1)} %all-to-all-done.1), channel_id=1, source_target_pairs={{0,16},{16,0},{1,17},{17,1},{2,18},{18,2},{3,19},{19,3},{4,20},{20... | collective-permute-start | bytes 1572872 | tf_op jit(solution)/shard_map/ppermute | solution.py:25
  306.0 21.7 %collective-permute-start.12 = (f32[256,1024]{1,0:T(8,128)}, f32[256,1024]{1,0:T(8,128)}, u32[]{:S(2)}, u32[]{:S(2)}) collective-permute-start(f32[256,1024]{1,0:T(8,128)} %pad_maximum_fusion.3), channel_id=1, source_target_pairs={{0,1},{1,0},{2,3},{3,2},{4,5},{5,4},{6,7},{7,6},{8,9},{9,8},{10,11... | collective-permute-start | bytes 3145736 | tf_op jit(solution)/shard_map/ppermute | solution.py:25
  307.4 3.7 %collective-permute-start.16 = (f32[2048]{0:T(1024)S(1)}, f32[2048]{0:T(1024)S(1)}, u32[]{:S(2)}, u32[]{:S(2)}) collective-permute-start(f32[2048]{0:T(1024)S(1)} %bitcast.178), channel_id=1, source_target_pairs={{0,2},{2,0},{4,6},{6,4},{8,10},{10,8},{12,14},{14,12},{1,3},{3,1},... | collective-permute-start | bytes 24584 | tf_op jit(solution)/shard_map/ppermute | solution.py:91
  309.2 14.0 %collective-permute-start.15 = (f32[256]{0:T(256)S(1)}, f32[256]{0:T(256)S(1)}, u32[]{:S(2)}, u32[]{:S(2)}) collective-permute-start(f32[256]{0:T(256)S(1)} %bitcast.180), channel_id=1, source_target_pairs={{0,1},{1,0},{2,3},{3,2},{4,5},{5,4},{6,7},{7,6},{8,9},{9,8},{10,11... | collective-permute-start | bytes 3080 | tf_op jit(solution)/shard_map/ppermute | solution.py:91
  311.1 11.4 %collective-permute-start.17 = (f32[2048]{0:T(1024)S(1)}, f32[2048]{0:T(1024)S(1)}, u32[]{:S(2)}, u32[]{:S(2)}) collective-permute-start(f32[2048]{0:T(1024)S(1)} %add.165), channel_id=1, source_target_pairs={{0,4},{2,6},{4,0},{6,2},{8,12},{10,14},{12,8},{14,10},{1,5},{3,7},... | collective-permute-start | bytes 24584 | tf_op jit(solution)/shard_map/ppermute | solution.py:91
  315.9 3.2 copy-start.5
  322.6 4.6 %collective-permute-start.18 = (f32[2048]{0:T(1024)S(1)}, f32[2048]{0:T(1024)S(1)}, u32[]{:S(2)}, u32[]{:S(2)}) collective-permute-start(f32[2048]{0:T(1024)S(1)} %add.166), channel_id=1, source_target_pairs={{0,8},{2,10},{4,12},{6,14},{8,0},{10,2},{12,4},{14,6},{1,9},{3,11}... | collective-permute-start | bytes 24584 | tf_op jit(solution)/shard_map/ppermute | solution.py:91
  332.8 2.2 copy-start.1
Sparse Core Ops, SparseCore 0:
  10.7 94.6 all-gather.4
  108.1 72.8 all-gather.6
where the time goes:
time: 343 us; the launch traced here: 342 us
  waiting for transfers between devices  169 us (49%)
  blocking collectives  49.7 us (14%)
  matrix products  33.8 us (10%)
  starting transfers between devices  33.4 us (10%)
  local copies, waits for them, and re-layouts  23.4 us (7%)
  other arithmetic  18.4 us (5%)
  between operations  14.4 us (4%)
    all_gather x1, waiting for transfers between devices, token_plan(): lax.all_gather(own_block(cotangent.reshape(cores, rows // cores, width),...  68.6 us
    all_to_all x1, blocking collectives, exchange(): return lax.all_to_all(blocks, axis, 0, 0)  49.7 us
    ppermute x7, waiting for transfers between devices, rotate(): lax.ppermute(block, axis, [(at, (at + shift) % size) for at in range(size)])  36.9 us
    dot_general x6, matrix products, contract(): lax.dot_general(left, right, (((left_dim,), (right_dim,)), ((), ())), pre...  33.8 us
    ppermute x2, waiting for transfers between devices, fs_sum(): got = lax.ppermute(near_block(shift).astype(NARROW), 'fs', perm)  22 us
    all_gather x1, waiting for transfers between devices, token_plan(): lax.all_gather(own_block(inputs.reshape(cores, rows // cores, width), 'tp...  18.6 us
    ppermute x6, waiting for transfers between devices, fs_sum(): got = lax.ppermute(far_block(shift).astype(NARROW), 'fs', perm)  17.6 us
    ppermute x6, starting transfers between devices, fs_sum(): got = lax.ppermute(far_block(shift).astype(NARROW), 'fs', perm)  10.6 us
  transfers between devices with their start and end apart: 23, of which 12 were waited for; matrix products, arithmetic and copies ran while one was open for 16% of the time, Pallas kernels for 0%

commit v1 on v0

--- a/solution.py
+++ b/solution.py
@@ -1,6 +1,10 @@
+import functools
+
 import jax
 import jax.numpy as jnp
 from jax import lax
+from jax.experimental import pallas as pl
+from jax.experimental.pallas import tpu as pltpu
 from jax.sharding import PartitionSpec as P
 
 NARROW = jnp.bfloat16
@@ -175,10 +179,500 @@
     return (grad_inputs, grad_up, grad_down, norms_up, norms_down)
 
 
+MESH = pl.DeviceIdType.MESH
+SPLITS = 2
+
+
+def dot(left, right, left_dim, right_dim):
+    return lax.dot_general(
+        left, right, (((left_dim,), (right_dim,)), ((), ())), preferred_element_type=jnp.float32
+    )
+
+
+class Slots:
+    def __init__(self):
+        self.size = 0
+        self.base = {}
+
+    def add(self, name, *shape):
+        self.base[name] = (self.size, shape)
+        count = 1
+        for extent in shape:
+            count *= extent
+        self.size += count
+
+    def at(self, name, *index):
+        start, shape = self.base[name]
+        place = 0
+        for extent, position in zip(shape, index, strict=True):
+            place = place * extent + position
+        return start + place
+
+
+def plane_slots(lines, splits):
+    sent, got, local = Slots(), Slots(), Slots()
+    for table in (sent, got):
+        table.add("pair", splits, 2)
+        table.add("near_x", 2, 2)
+        table.add("near_y", 2, 2)
+        table.add("far", 2, 2)
+        table.add("core_tokens", 2, 3)
+        table.add("core_up", splits, lines)
+        table.add("core_pre", splits)
+        table.add("spread_y", splits, 2)
+        table.add("spread_x", splits, 2, 2)
+        table.add("share", 3)
+        table.add("core_share")
+        table.add("reduce_up", splits, 2, lines)
+        table.add("reduce_down", splits, 2, lines)
+    sent.add("line_up", splits, 2, 2, lines)
+    sent.add("line_down", splits, 2, 2, lines)
+    got.add("line", splits, 2, 2, lines)
+    local.add("tokens", 2)
+    local.add("weights", splits, 2)
+    local.add("share")
+    local.add("out", 2)
+    return sent, got, local
+
+
+def plane_kernel(
+    lines, splits, sent, got, local,
+    tokens_hbm, cot_hbm, up_hbm, down_hbm,
+    share_out, up_out, down_out,
+    tokens, cots, ups, downs, other_up, pre_act, act_grad, pre_grad, other_pre, turned,
+    leaving, rising, falling, partial, spread, spread_far, share_leaving, share_got, share_sum,
+    send_sems, got_sems, local_sems,
+):
+    rows, width = tokens_hbm.shape
+    depth, units = up_hbm.shape
+    mine = units // 4
+    step = mine // splits
+    wide = 2 * depth
+    half = rows // 2
+    bit = half // 2
+    near = lines // 2
+    mid = width // 2
+
+    x = lax.axis_index("rep")
+    fs = lax.axis_index("fs")
+    core = lax.axis_index("tp")
+    z, y = fs // 2, fs % 2
+    me = 2 * x + y
+    at_x, at_y, at_far = 2 * (1 - x) + y, 2 * x + 1 - y, 2 * (1 - x) + 1 - y
+    to_x = (1 - x, fs, core)
+    to_y = (x, 2 * z + 1 - y, core)
+    to_far = (1 - x, 2 * z + 1 - y, core)
+    to_core = (x, fs, 1 - core)
+    to_up = (x, fs + 2, core)
+    to_down = (x, fs - 2, core)
+    has_up, has_down = z < lines - 1, z > 0
+    pending = []
+
+    def when(cond, act):
+        if cond is None:
+            act()
+        else:
+            pl.when(cond)(act)
+
+    def send(src, dst, sem, to, key, *index, cond=None, got_key=None):
+        copy = pltpu.make_async_remote_copy(
+            src_ref=src, dst_ref=dst,
+            send_sem=send_sems.at[sent.at(key, *index)],
+            recv_sem=got_sems.at[got.at(got_key or key, *index)],
+            device_id=to, device_id_type=MESH,
+        )
+        when(cond, copy.start)
+        pending.append((cond, copy))
+
+    def arrived(dst, key, *index):
+        return pltpu.make_async_remote_copy(
+            src_ref=dst, dst_ref=dst, send_sem=send_sems.at[0],
+            recv_sem=got_sems.at[got.at(key, *index)],
+            device_id=to_core, device_id_type=MESH,
+        )
+
+    def fetch(src, dst, key, *index):
+        copy = pltpu.make_async_copy(src, dst, local_sems.at[local.at(key, *index)])
+        copy.start()
+        return copy
+
+    def up_piece(k, line, side):
+        return ups.at[k, line, pl.ds(pl.multiple_of(side * depth, depth), depth), :]
+
+    def down_piece(k, line, side):
+        return downs.at[k, line, :, pl.ds(pl.multiple_of(side * depth, depth), depth)]
+
+    def piece(w, k, line, side):
+        return (up_piece, down_piece)[w](k, line, side)
+
+    def own(w, owner, k):
+        at = pl.ds(pl.multiple_of(owner * mine + k * step, step), step)
+        return up_hbm.at[:, at] if w == 0 else down_hbm.at[at, :]
+
+    def band(t, owner, first, count):
+        return (tokens, cots)[t].at[pl.ds(pl.multiple_of(owner * rows + first, bit), count), :]
+
+    gets = {}
+    for k in range(splits):
+        for w in range(2):
+            gets[k, w] = fetch(own(w, me, k), piece(w, k, z, y), "weights", k, w)
+        if k == 0:
+            for t, src in ((0, tokens_hbm), (1, cot_hbm)):
+                gets[t] = fetch(src, band(t, me, 0, rows), "tokens", t)
+
+    barrier = pltpu.get_barrier_semaphore()
+    for to in (to_x, to_y, to_far, to_core):
+        pl.semaphore_signal(barrier, inc=1, device_id=to, device_id_type=MESH)
+
+    @pl.when(has_up)
+    def _():
+        pl.semaphore_signal(barrier, inc=1, device_id=to_up, device_id_type=MESH)
+
+    @pl.when(has_down)
+    def _():
+        pl.semaphore_signal(barrier, inc=1, device_id=to_down, device_id_type=MESH)
+
+    pl.semaphore_wait(barrier, 4 + has_up.astype(jnp.int32) + has_down.astype(jnp.int32))
+
+    def pair_send(k):
+        for w in range(2):
+            send(own(w, at_y, k), piece(w, k, z, y), None, to_y, "pair", k, w)
+
+    def line_send(k, side):
+        for w in range(2):
+            ref = piece(w, k, z, side)
+            send(ref, ref, None, to_up, "line_up", k, w, side, z, cond=has_up, got_key="line")
+            send(ref, ref, None, to_down, "line_down", k, w, side, z, cond=has_down, got_key="line")
+
+    def pair_wait(k):
+        for w in range(2):
+            arrived(piece(w, k, z, 1 - y), "pair", k, w).wait_recv()
+
+    first = core * half
+
+    def near_send(t):
+        for p in range(2):
+            ref = band(t, me, first + p * bit, bit)
+            send(ref, ref, None, to_x, "near_x", t, p)
+            ref = band(t, me, first + (1 - p) * bit, bit)
+            send(ref, ref, None, to_y, "near_y", t, 1 - p)
+
+    def relay(t):
+        ref = band(t, at_x, first, bit)
+        arrived(ref, "near_x", t, 0).wait_recv()
+        send(ref, ref, None, to_y, "far", t, 0)
+        ref = band(t, at_y, first + bit, bit)
+        arrived(ref, "near_y", t, 1).wait_recv()
+        send(ref, ref, None, to_x, "far", t, 1)
+        arrived(band(t, at_x, first + bit, bit), "near_x", t, 1).wait_recv()
+        arrived(band(t, at_y, first, bit), "near_y", t, 0).wait_recv()
+        for i, owner in enumerate((at_x, at_y)):
+            ref = band(t, owner, first, half)
+            send(ref, ref, None, to_core, "core_tokens", t, i)
+
+    def far_wait(t):
+        for p in range(2):
+            arrived(band(t, at_far, first + p * bit, bit), "far", t, p).wait_recv()
+        ref = band(t, at_far, first, half)
+        send(ref, ref, None, to_core, "core_tokens", t, 2)
+
+    def core_wait(t):
+        for i, owner in enumerate((at_x, at_y, at_far)):
+            arrived(band(t, owner, (1 - core) * half, half), "core_tokens", t, i).wait_recv()
+
+    def core_up_send(k, line, cond):
+        other = (1 - core) * near
+        inside = jnp.logical_and(line >= other, line < other + near)
+        if cond is not None:
+            inside = jnp.logical_and(inside, cond)
+        send(ups.at[k, line], other_up.at[k, line], None, to_core, "core_up", k, line, cond=inside)
+
+    def from_line(k, line, cond, onward, to, key):
+        for w in range(2):
+            for side in range(2):
+                ref = piece(w, k, line, side)
+                when(cond, arrived(ref, "line", k, w, side, line).wait_recv)
+                send(
+                    ref, ref, None, to, key, k, w, side, line,
+                    cond=jnp.logical_and(cond, onward), got_key="line",
+                )
+        core_up_send(k, line, cond)
+
+    def forward(k, line, fresh):
+        cols = pl.ds(pl.multiple_of(line * wide, wide), wide)
+        a = dot(tokens[:, cols], ups[k, line], 1, 0)
+        pre_act[...] = a if fresh else pre_act[...] + a
+
+    def backward(k, line, fresh):
+        cols = pl.ds(pl.multiple_of(line * wide, wide), wide)
+        a = dot(cots[:, cols], downs[k, line], 1, 1)
+        act_grad[...] = a if fresh else act_grad[...] + a
+
+    def gather_step(k, d, compute):
+        below, above = z - d, z + d
+        for line, cond, onward, to, key in (
+            (below, below >= 0, has_up, to_up, "line_up"),
+            (above, above < lines, has_down, to_down, "line_down"),
+        ):
+            at = lax.rem(line + lines, lines)
+            from_line(k, at, cond, onward, to, key)
+            if compute:
+
+                @pl.when(cond)
+                def _():
+                    forward(k, at, False)
+                    backward(k, at, False)
+
+    def activate(k):
+        def body(i, carry):
+            at = pl.ds(pl.multiple_of(i * rows, rows), rows)
+            r = jnp.maximum(pre_act[at, :], 0.0)
+            g = (2.0 * r * act_grad[at, :]).astype(jnp.bfloat16)
+            pre_grad[k, at, :] = g
+            turned[k, 0, :, at] = g.T
+            turned[k, 1, :, at] = (r * r).astype(jnp.bfloat16).T
+            return carry
+
+        lax.fori_loop(0, 4, body, 0)
+        send(pre_grad.at[k], other_pre.at[k], None, to_core, "core_pre", k)
+
+    def term(k, w, owner):
+        cols = pl.ds(pl.multiple_of(owner * wide, wide), wide)
+        return dot(turned[k, w], (tokens, cots)[w][:, cols], 1, 0)
+
+    def reduce_to(k, w, owner, cond, has_in, inbox, in_key, to):
+        at = lax.rem(owner + lines, lines)
+        box = inbox.at[k, w, at]
+        wait = arrived(box, in_key, k, w, at)
+        out = leaving.at[k, w, at]
+
+        @pl.when(cond)
+        def _():
+            partial[...] = term(k, w, at)
+
+            @pl.when(has_in)
+            def _():
+                wait.wait_recv()
+                out[...] = (partial[...] + box[...].astype(jnp.float32)).astype(jnp.bfloat16)
+
+            @pl.when(jnp.logical_not(has_in))
+            def _():
+                out[...] = partial[...].astype(jnp.bfloat16)
+
+        send(out, box, None, to, in_key, k, w, at, cond=cond)
+
+    def reduce_step(k, w, i):
+        reduce_to(k, w, lines - 1 - i, z < lines - 1 - i, has_down, rising, "reduce_up", to_up)
+        reduce_to(k, w, i + 0 * z, z > i, has_up, falling, "reduce_down", to_down)
+
+    def reduce_own(k, w):
+        partial[...] = term(k, w, z)
+        for cond, inbox, key in ((has_down, rising, "reduce_up"), (has_up, falling, "reduce_down")):
+            box = inbox.at[k, w, z]
+            wait = arrived(box, key, k, w, z)
+
+            @pl.when(cond)
+            def _():
+                wait.wait_recv()
+                partial[...] += box[...].astype(jnp.float32)
+
+        here = spread.at[w, me, k]
+        here[...] = partial[:, pl.ds(pl.multiple_of(y * depth, depth), depth)].astype(jnp.bfloat16)
+        there = spread_far.at[k, w]
+        there[...] = partial[:, pl.ds(pl.multiple_of((1 - y) * depth, depth), depth)].astype(jnp.bfloat16)
+        send(there, here, None, to_y, "spread_y", k, w)
+        send(here, here, None, to_x, "spread_x", k, w, 0)
+
+    def spread_relay(k, w):
+        ref = spread.at[w, at_y, k]
+        arrived(ref, "spread_y", k, w).wait_recv()
+        send(ref, ref, None, to_x, "spread_x", k, w, 1)
+
+    def spread_wait(k, w):
+        arrived(spread.at[w, at_x, k], "spread_x", k, w, 0).wait_recv()
+        arrived(spread.at[w, at_far, k], "spread_x", k, w, 1).wait_recv()
+
+    def share_term(owner):
+        at = pl.ds(pl.multiple_of(owner * rows, rows), rows)
+        parts = []
+        for i in range(near):
+            line = core * near + i
+            total = None
+            for k in range(splits):
+                for grads, weights in ((pre_grad, ups), (other_pre, other_up)):
+                    a = dot(grads[k, at, :], weights[k, line], 1, 1)
+                    total = a if total is None else total + a
+            parts.append(total)
+        return parts
+
+    def share_send():
+        for k in range(splits):
+            arrived(other_pre.at[k], "core_pre", k).wait_recv()
+            for i in range(near):
+                line = core * near + i
+                arrived(other_up.at[k, line], "core_up", k, line).wait_recv()
+        for j, (owner, to) in enumerate(((at_far, to_far), (at_x, to_x), (at_y, to_y))):
+            for i, part in enumerate(share_term(owner)):
+                share_leaving[j, :, i * wide : (i + 1) * wide] = part.astype(jnp.bfloat16)
+            send(share_leaving.at[j], share_got.at[j], None, to, "share", j)
+        for i, part in enumerate(share_term(me)):
+            share_sum[:, i * wide : (i + 1) * wide] = part
+
+    def share_end():
+        for j in range(3):
+            arrived(share_got.at[j], "share", j).wait_recv()
+            share_sum[...] += share_got[j].astype(jnp.float32)
+        place = share_out.at[:, pl.ds(pl.multiple_of(core * mid, mid), mid)]
+        send(share_sum, place, None, to_core, "core_share")
+        return fetch(share_sum, place, "share")
+
+    pair_send(0)
+    for w in range(2):
+        gets[0, w].wait()
+    line_send(0, y)
+    gets[0].wait()
+    near_send(0)
+    for k in range(1, splits):
+        pair_send(k)
+    gets[1].wait()
+    near_send(1)
+    pair_wait(0)
+    line_send(0, 1 - y)
+    core_up_send(0, z, None)
+    for k in range(1, splits):
+        for w in range(2):
+            gets[k, w].wait()
+        line_send(k, y)
+    relay(0)
+    gather_step(0, 1, False)
+    for k in range(1, splits):
+        pair_wait(k)
+        line_send(k, 1 - y)
+        core_up_send(k, z, None)
+    far_wait(0)
+    relay(1)
+    for d in range(2, lines):
+        gather_step(0, d, False)
+    core_wait(0)
+    for i in range(lines):
+        forward(0, lax.rem(z + i, lines), i == 0)
+    far_wait(1)
+    core_wait(1)
+    for i in range(lines):
+        backward(0, lax.rem(z + i, lines), i == 0)
+
+    for k in range(splits):
+        activate(k)
+        last = k == splits - 1
+        if last:
+            share_send()
+        steps = [functools.partial(reduce_step, k, w, i) for w in range(2) for i in range(lines - 1)]
+        steps.insert(lines, functools.partial(reduce_own, k, 0))
+        steps.append(functools.partial(reduce_own, k, 1))
+        fills = []
+        if not last:
+            def begin(k=k):
+                forward(k + 1, z, True)
+                backward(k + 1, z, True)
+
+            fills = [begin] + [functools.partial(gather_step, k + 1, d, True) for d in range(1, lines)]
+        every = max(1, len(steps) // max(1, len(fills)))
+        while steps or fills:
+            for _ in range(every):
+                if steps:
+                    steps.pop(0)()
+            if fills:
+                fills.pop(0)()
+        for w in range(2):
+            spread_relay(k, w)
+
+    out = share_end()
+    for k in range(splits):
+        for w in range(2):
+            spread_wait(k, w)
+    ends = [fetch(spread.at[w], ref, "out", w) for w, ref in enumerate((up_out, down_out))]
+    arrived(share_out.at[:, pl.ds(pl.multiple_of((1 - core) * mid, mid), mid)], "core_share").wait_recv()
+    for cond, copy in pending:
+        when(cond, copy.wait_send)
+    out.wait()
+    for end in ends:
+        end.wait()
+
+
+def plane_fits(inputs, up_weight, down_weight):
+    reps, groups, cores = (lax.axis_size(axis) for axis in ("rep", "fs", "tp"))
+    if reps != 2 or cores != 2 or groups % 4:
+        return False
+    rows, width = inputs.shape
+    depth, units = up_weight.shape
+    step = units // 4 // SPLITS
+    even = rows % 64 == 0 and depth % 128 == 0 and step % 128 == 0 and width == groups * depth
+    held = 2 * 4 * rows * width * 2 + 4 * (units // 4) * width * 2
+    return even and held <= 16 * 2**20
+
+
+def plane_plan(inputs, cotangent, up_weight, down_weight):
+    groups = lax.axis_size("fs")
+    lines, splits = groups // 2, SPLITS
+    rows, width = inputs.shape
+    depth, units = up_weight.shape
+    step = units // 4 // splits
+    wide = 2 * depth
+    plane = 4 * rows
+    sent, got, local = plane_slots(lines, splits)
+    narrow, full = jnp.bfloat16, jnp.float32
+    anywhere = pl.BlockSpec(memory_space=pl.ANY)
+    share, up, down = pl.pallas_call(
+        functools.partial(plane_kernel, lines, splits, sent, got, local),
+        out_shape=(
+            jax.ShapeDtypeStruct((rows, width), full),
+            jax.ShapeDtypeStruct((4, splits, step, depth), narrow),
+            jax.ShapeDtypeStruct((4, splits, step, depth), narrow),
+        ),
+        in_specs=[anywhere] * 4,
+        out_specs=(anywhere,) * 3,
+        scratch_shapes=[
+            pltpu.VMEM((plane, width), narrow),
+            pltpu.VMEM((plane, width), narrow),
+            pltpu.VMEM((splits, lines, wide, step), narrow),
+            pltpu.VMEM((splits, lines, step, wide), narrow),
+            pltpu.VMEM((splits, lines, wide, step), narrow),
+            pltpu.VMEM((plane, step), full),
+            pltpu.VMEM((plane, step), full),
+            pltpu.VMEM((splits, plane, step), narrow),
+            pltpu.VMEM((splits, plane, step), narrow),
+            pltpu.VMEM((splits, 2, step, plane), narrow),
+            pltpu.VMEM((splits, 2, lines, step, wide), narrow),
+            pltpu.VMEM((splits, 2, lines, step, wide), narrow),
+            pltpu.VMEM((splits, 2, lines, step, wide), narrow),
+            pltpu.VMEM((step, wide), full),
+            pltpu.VMEM((2, 4, splits, step, depth), narrow),
+            pltpu.VMEM((splits, 2, step, depth), narrow),
+            pltpu.VMEM((3, rows, width // 2), narrow),
+            pltpu.VMEM((3, rows, width // 2), narrow),
+            pltpu.VMEM((rows, width // 2), full),
+            pltpu.SemaphoreType.DMA((sent.size,)),
+            pltpu.SemaphoreType.DMA((got.size,)),
+            pltpu.SemaphoreType.DMA((local.size,)),
+        ],
+        compiler_params=pltpu.CompilerParams(
+            collective_id=0, has_side_effects=True, vmem_limit_bytes=63 * 2**20
+        ),
+        name="plane",
+    )(inputs, cotangent, up_weight, down_weight)
+    grad_up = up.reshape(units, depth).T.astype(full)
+    grad_down = down.reshape(units, depth).astype(full)
+    norms_up = small_sum(jnp.sum(grad_up * grad_up, axis=1), "tp")
+    norms_down = small_sum(jnp.sum(grad_down * grad_down, axis=1), "fs")
+    return (share, grad_up, grad_down, norms_up, norms_down)
+
+
 def shards(inputs, cotangent, up_weight, down_weight):
     tokens = inputs.size * lax.axis_size("fs") // lax.axis_size("tp")
     weights = up_weight.size * lax.axis_size("fs")
     plan = token_plan if tokens <= weights else weight_plan
+    if plane_fits(inputs, up_weight, down_weight):
+        plan = plane_plan
     return plan(inputs, cotangent, up_weight, down_weight)
 
 

time: 343 us -> 217 us (0.63)
  Pallas kernels: 0 us -> 198 us
  waiting for transfers between devices: 169 us -> 3.34 us
  blocking collectives: 49.7 us -> 0 us
  matrix products: 33.8 us -> 0 us
  starting transfers between devices: 33.4 us -> 4.34 us
  local copies, waits for them, and re-layouts: 23.4 us -> 3.26 us
  between operations: 14.4 us -> 0.72 us
  other arithmetic: 18.4 us -> 7.22 us
    pallas_call x0 -> x1, Pallas kernels: none -> 198 us  [plane_plan(): pl.pallas_call(functools.partial(plane_kernel, lines, splits, sent, got,...]
    all_gather x2 -> x0, waiting for transfers between devices: 87.2 us -> none  [the longest x1 68.6 us: token_plan(): lax.all_gather(own_block(cotangent.reshape(cores, rows // cores, width),...]
    ppermute x15 -> x0, waiting for transfers between devices: 76.6 us -> none  [the longest x7 36.9 us: rotate(): lax.ppermute(block, axis, [(at, (at + shift) % size) for at in range(size)])]
    all_to_all x1 -> x0, blocking collectives: 49.7 us -> none  [exchange(): return lax.all_to_all(blocks, axis, 0, 0)]
    dot_general x6 -> x0, matrix products: 33.8 us -> none  [contract(): lax.dot_general(left, right, (((left_dim,), (right_dim,)), ((), ())), pre...]
    ppermute x15 -> x0, starting transfers between devices: 21.3 us -> none  [the longest x6 10.6 us: fs_sum(): got = lax.ppermute(far_block(shift).astype(NARROW), 'fs', perm)]
    all_to_all x2 -> x0, starting transfers between devices: 9.76 us -> none  [exchange(): return lax.all_to_all(blocks, axis, 0, 0)]
    unnamed x28 -> x8, local copies, waits for them, and re-layouts: 10.5 us -> 1.34 us
  transfers between devices with their start and end apart: 23 -> 4, of which waited for: 12 -> 1; matrix products, arithmetic and copies ran while one was open for 16% -> 3% of each run, Pallas kernels for 0% -> 0%
where the time goes in v1:
time: 217 us
  Pallas kernels  198 us (91%)
  other arithmetic  7.22 us (3%)
  starting transfers between devices  4.34 us (2%)
  waiting for transfers between devices  3.34 us (2%)
  local copies, waits for them, and re-layouts  3.26 us (2%)
    pallas_call x1, Pallas kernels, plane_plan(): pl.pallas_call(functools.partial(plane_kernel, lines, splits, sent, got,...  198 us
    ppermute x4, starting transfers between devices, small_sum(): lax.ppermute(value, axis, [(at, at ^ bit) for at in range(size)])  4.34 us
  transfers between devices with their start and end apart: 4, of which 1 were waited for; matrix products, arithmetic and copies ran while one was open for 3% of the time, Pallas kernels for 0%

profile of v1, /device:TPU:0, one launch (start us, length us, event | category | flops | bytes accessed | tf_op | source)
XLA Modules:
  0.0 216.5 jit_solution(17670674365657556095)
XLA Ops:
  0.6 197.6 %plane.1 = (f32[256,2048]{1,0:T(8,128)}, bf16[4,2,256,256]{3,2,1,0:T(8,128)(2,1)}, bf16[4,2,256,256]{3,2,1,0:T(8,128)(2,1)}) custom-call(bf16[256,2048]{1,0:T(8,128)(2,1)} %tokens_hbm.1, bf16[256,2048]{1,0:T(8,128)(2,1)} %cot_hbm.1, bf16[256,2048]{1,0:T(8,128)(2,1)} %up_hbm.1, bf16[2048,256]{1,0:T(8,128)(2,1)} %down_hbm.1), custom_call_target="tpu_custom_call" | custom-call | tf_op jit(solution)/shard_map/plane/pallas_call | solution.py:625
  198.3 1.6 multiply_reduce_fusion
  199.9 1.6 collective-permute-start.1
  201.5 2.7 %bitcast_convert_fusion = f32[2048,256]{1,0:T(8,128)} fusion(bf16[4,2,256,256]{3,2,1,0:T(8,128)(2,1)} %get-tuple-element.9), kind=kLoop, calls=%fused_computation.2 | loop fusion | flops 524288 | bytes 3145728 | tf_op jit(solution)/shard_map/convert_element_type | solution.py:663
  204.2 1.9 copy.9
  206.1 0.0 copy-start
  206.1 0.0 copy-start.1
  206.1 0.0 collective-permute-done.1
  206.1 0.1 collective-permute-start.2
  206.2 0.2 multiply_reduce_fusion.1
  206.4 0.0 copy-start.2
  206.4 0.1 collective-permute-start
  206.5 3.3 %collective-permute-done.2 = f32[2048]{0:T(1024)S(1)} collective-permute-done((f32[2048]{0:T(1024)S(1)}, f32[2048]{0:T(1024)S(1)}, u32[]{:S(2)}, u32[]{:S(2)}) %collective-permute-start.2) | collective-permute-done | bytes 8224 | tf_op jit(solution)/shard_map/ppermute | solution.py:95
  209.8 2.6 %collective-permute-start.3 = (f32[2048]{0:T(1024)S(1)}, f32[2048]{0:T(1024)S(1)}, u32[]{:S(2)}, u32[]{:S(2)}) collective-permute-start(f32[2048]{0:T(1024)S(1)} %add.14), channel_id=1, source_target_pairs={{0,8},{2,10},{4,12},{6,14},{8,0},{10,2},{12,4},{14,6},{1,9},{3,11}... | collective-permute-start | bytes 24584 | tf_op jit(solution)/shard_map/ppermute | solution.py:95
  212.5 0.0 copy-done.1
  212.5 1.5 bitcast_convert_fusion.1
  214.0 0.0 copy-done
  214.0 0.0 collective-permute-done
  214.0 0.6 add.12
  214.6 0.0 collective-permute-done.3
  214.6 0.6 add.15
  215.2 0.0 copy-done.2
  215.2 1.3 copy.12
  (3 shorter events, 0.0 us)
Async XLA Ops:
  199.9 6.2 %collective-permute-start.1 = (f32[2048]{0:T(1024)S(1)}, f32[2048]{0:T(1024)S(1)}, u32[]{:S(2)}, u32[]{:S(2)}) collective-permute-start(f32[2048]{0:T(1024)S(1)} %bitcast.12), channel_id=1, source_target_pairs={{0,2},{2,0},{4,6},{6,4},{8,10},{10,8},{12,14},{14,12},{1,3},{3,1},... | collective-permute-start | bytes 24584 | tf_op jit(solution)/shard_map/ppermute | solution.py:95
  206.1 7.9 %copy-start = (f32[2048,256]{0,1:T(8,128)}, f32[2048,256]{0,1:T(8,128)S(1)}, u32[]{:S(2)}) copy-start(f32[2048,256]{0,1:T(8,128)S(1)} %copy.9) | copy-start | bytes 6291460
  206.1 6.4 %copy-start.1 = (bf16[4,2,256,256]{3,2,1,0:T(8,128)(2,1)S(1)}, bf16[4,2,256,256]{3,2,1,0:T(8,128)(2,1)}, u32[]{:S(2)}) copy-start(bf16[4,2,256,256]{3,2,1,0:T(8,128)(2,1)} %get-tuple-element.10) | copy-start | bytes 3145732
  206.1 3.7 %collective-permute-start.2 = (f32[2048]{0:T(1024)S(1)}, f32[2048]{0:T(1024)S(1)}, u32[]{:S(2)}, u32[]{:S(2)}) collective-permute-start(f32[2048]{0:T(1024)S(1)} %add.13), channel_id=1, source_target_pairs={{0,4},{2,6},{4,0},{6,2},{8,12},{10,14},{12,8},{14,10},{1,5},{3,7},... | collective-permute-start | bytes 24584 | tf_op jit(solution)/shard_map/ppermute | solution.py:95
  206.4 8.8 %copy-start.2 = (f32[256,2048]{1,0:T(8,128)S(1)}, f32[256,2048]{1,0:T(8,128)}, u32[]{:S(2)}) copy-start(f32[256,2048]{1,0:T(8,128)} %get-tuple-element.16) | copy-start | bytes 6291460
  206.4 7.6 %collective-permute-start = (f32[256]{0:T(256)S(1)}, f32[256]{0:T(256)S(1)}, u32[]{:S(2)}, u32[]{:S(2)}) collective-permute-start(f32[256]{0:T(256)S(1)} %multiply_reduce_fusion.1), channel_id=1, source_target_pairs={{0,1},{1,0},{2,3},{3,2},{4,5},{5,4},{6,7},{7,6},{8,9},{9,8},{10,11... | collective-permute-start | bytes 3080 | tf_op jit(solution)/shard_map/ppermute | solution.py:95
  209.8 4.7 %collective-permute-start.3 = (f32[2048]{0:T(1024)S(1)}, f32[2048]{0:T(1024)S(1)}, u32[]{:S(2)}, u32[]{:S(2)}) collective-permute-start(f32[2048]{0:T(1024)S(1)} %add.14), channel_id=1, source_target_pairs={{0,8},{2,10},{4,12},{6,14},{8,0},{10,2},{12,4},{14,6},{1,9},{3,11}... | collective-permute-start | bytes 24584 | tf_op jit(solution)/shard_map/ppermute | solution.py:95

commit v2 on v1

--- a/solution.py
+++ b/solution.py
@@ -223,8 +223,7 @@
         table.add("spread_x", splits, 2, 2)
         table.add("share", 3)
         table.add("core_share")
-        table.add("reduce_up", splits, 2, lines)
-        table.add("reduce_down", splits, 2, lines)
+        table.add("reduce", 2, splits, 2, lines)
     sent.add("line_up", splits, 2, 2, lines)
     sent.add("line_down", splits, 2, 2, lines)
     got.add("line", splits, 2, 2, lines)
@@ -239,8 +238,8 @@
     lines, splits, sent, got, local,
     tokens_hbm, cot_hbm, up_hbm, down_hbm,
     share_out, up_out, down_out,
-    tokens, cots, ups, downs, other_up, pre_act, act_grad, pre_grad, other_pre, turned,
-    leaving, rising, falling, partial, spread, spread_far, share_leaving, share_got, share_sum,
+    acts, ups, downs, other_up, pre_act, act_grad, pre_grad, other_pre, turned,
+    leaving, inbox, partial, spread, spread_far, share_leaving, share_got, share_sum,
     send_sems, got_sems, local_sems,
 ):
     rows, width = tokens_hbm.shape
@@ -266,6 +265,8 @@
     to_up = (x, fs + 2, core)
     to_down = (x, fs - 2, core)
     has_up, has_down = z < lines - 1, z > 0
+    middle = jnp.logical_and(has_up, has_down)
+    end = jnp.logical_not(middle)
     pending = []
 
     def when(cond, act):
@@ -274,13 +275,16 @@
         else:
             pl.when(cond)(act)
 
-    def send(src, dst, sem, to, key, *index, cond=None, got_key=None):
-        copy = pltpu.make_async_remote_copy(
+    def remote(src, dst, to, key, *index, got_key=None):
+        return pltpu.make_async_remote_copy(
             src_ref=src, dst_ref=dst,
             send_sem=send_sems.at[sent.at(key, *index)],
             recv_sem=got_sems.at[got.at(got_key or key, *index)],
             device_id=to, device_id_type=MESH,
         )
+
+    def send(src, dst, to, key, *index, cond=None, got_key=None):
+        copy = remote(src, dst, to, key, *index, got_key=got_key)
         when(cond, copy.start)
         pending.append((cond, copy))
 
@@ -310,7 +314,7 @@
         return up_hbm.at[:, at] if w == 0 else down_hbm.at[at, :]
 
     def band(t, owner, first, count):
-        return (tokens, cots)[t].at[pl.ds(pl.multiple_of(owner * rows + first, bit), count), :]
+        return acts.at[t, pl.ds(pl.multiple_of(owner * rows + first, bit), count), :]
 
     gets = {}
     for k in range(splits):
@@ -336,13 +340,16 @@
 
     def pair_send(k):
         for w in range(2):
-            send(own(w, at_y, k), piece(w, k, z, y), None, to_y, "pair", k, w)
-
-    def line_send(k, side):
+            send(own(w, at_y, k), piece(w, k, z, y), to_y, "pair", k, w)
+
+    def line_send(k, side, who=None):
+        up_cond, down_cond = has_up, has_down
+        if who is not None:
+            up_cond, down_cond = jnp.logical_and(has_up, who), jnp.logical_and(has_down, who)
         for w in range(2):
             ref = piece(w, k, z, side)
-            send(ref, ref, None, to_up, "line_up", k, w, side, z, cond=has_up, got_key="line")
-            send(ref, ref, None, to_down, "line_down", k, w, side, z, cond=has_down, got_key="line")
+            send(ref, ref, to_up, "line_up", k, w, side, z, cond=up_cond, got_key="line")
+            send(ref, ref, to_down, "line_down", k, w, side, z, cond=down_cond, got_key="line")
 
     def pair_wait(k):
         for w in range(2):
@@ -353,28 +360,28 @@
     def near_send(t):
         for p in range(2):
             ref = band(t, me, first + p * bit, bit)
-            send(ref, ref, None, to_x, "near_x", t, p)
+            send(ref, ref, to_x, "near_x", t, p)
             ref = band(t, me, first + (1 - p) * bit, bit)
-            send(ref, ref, None, to_y, "near_y", t, 1 - p)
+            send(ref, ref, to_y, "near_y", t, 1 - p)
 
     def relay(t):
         ref = band(t, at_x, first, bit)
         arrived(ref, "near_x", t, 0).wait_recv()
-        send(ref, ref, None, to_y, "far", t, 0)
+        send(ref, ref, to_y, "far", t, 0)
         ref = band(t, at_y, first + bit, bit)
         arrived(ref, "near_y", t, 1).wait_recv()
-        send(ref, ref, None, to_x, "far", t, 1)
+        send(ref, ref, to_x, "far", t, 1)
         arrived(band(t, at_x, first + bit, bit), "near_x", t, 1).wait_recv()
         arrived(band(t, at_y, first, bit), "near_y", t, 0).wait_recv()
         for i, owner in enumerate((at_x, at_y)):
             ref = band(t, owner, first, half)
-            send(ref, ref, None, to_core, "core_tokens", t, i)
+            send(ref, ref, to_core, "core_tokens", t, i)
 
     def far_wait(t):
         for p in range(2):
             arrived(band(t, at_far, first + p * bit, bit), "far", t, p).wait_recv()
         ref = band(t, at_far, first, half)
-        send(ref, ref, None, to_core, "core_tokens", t, 2)
+        send(ref, ref, to_core, "core_tokens", t, 2)
 
     def core_wait(t):
         for i, owner in enumerate((at_x, at_y, at_far)):
@@ -385,43 +392,46 @@
         inside = jnp.logical_and(line >= other, line < other + near)
         if cond is not None:
             inside = jnp.logical_and(inside, cond)
-        send(ups.at[k, line], other_up.at[k, line], None, to_core, "core_up", k, line, cond=inside)
-
-    def from_line(k, line, cond, onward, to, key):
-        for w in range(2):
-            for side in range(2):
-                ref = piece(w, k, line, side)
-                when(cond, arrived(ref, "line", k, w, side, line).wait_recv)
-                send(
-                    ref, ref, None, to, key, k, w, side, line,
-                    cond=jnp.logical_and(cond, onward), got_key="line",
-                )
-        core_up_send(k, line, cond)
+        send(ups.at[k, line], other_up.at[k, line], to_core, "core_up", k, line, cond=inside)
+
+    def beside(d):
+        below, above = z - d, z + d
+        return (
+            (lax.rem(below + lines, lines), below >= 0, has_up, to_up, "line_up"),
+            (lax.rem(above, lines), above < lines, has_down, to_down, "line_down"),
+        )
+
+    def gather_step(k, d, who=None):
+        for line, cond, onward, to, key in beside(d):
+            if who is not None:
+                cond = jnp.logical_and(cond, who)
+            for w in range(2):
+                for side in range(2):
+                    ref = piece(w, k, line, side)
+                    when(cond, arrived(ref, "line", k, w, side, line).wait_recv)
+                    send(
+                        ref, ref, to, key, k, w, side, line,
+                        cond=jnp.logical_and(cond, onward), got_key="line",
+                    )
+            core_up_send(k, line, cond)
 
     def forward(k, line, fresh):
         cols = pl.ds(pl.multiple_of(line * wide, wide), wide)
-        a = dot(tokens[:, cols], ups[k, line], 1, 0)
+        a = dot(acts[0, :, cols], ups[k, line], 1, 0)
         pre_act[...] = a if fresh else pre_act[...] + a
 
     def backward(k, line, fresh):
         cols = pl.ds(pl.multiple_of(line * wide, wide), wide)
-        a = dot(cots[:, cols], downs[k, line], 1, 1)
+        a = dot(acts[1, :, cols], downs[k, line], 1, 1)
         act_grad[...] = a if fresh else act_grad[...] + a
 
-    def gather_step(k, d, compute):
-        below, above = z - d, z + d
-        for line, cond, onward, to, key in (
-            (below, below >= 0, has_up, to_up, "line_up"),
-            (above, above < lines, has_down, to_down, "line_down"),
-        ):
-            at = lax.rem(line + lines, lines)
-            from_line(k, at, cond, onward, to, key)
-            if compute:
-
-                @pl.when(cond)
-                def _():
-                    forward(k, at, False)
-                    backward(k, at, False)
+    def compute_step(k, d):
+        for line, cond, _, _, _ in beside(d):
+
+            @pl.when(cond)
+            def _():
+                forward(k, line, False)
+                backward(k, line, False)
 
     def activate(k):
         def body(i, carry):
@@ -434,59 +444,90 @@
             return carry
 
         lax.fori_loop(0, 4, body, 0)
-        send(pre_grad.at[k], other_pre.at[k], None, to_core, "core_pre", k)
+        send(pre_grad.at[k], other_pre.at[k], to_core, "core_pre", k)
 
     def term(k, w, owner):
         cols = pl.ds(pl.multiple_of(owner * wide, wide), wide)
-        return dot(turned[k, w], (tokens, cots)[w][:, cols], 1, 0)
-
-    def reduce_to(k, w, owner, cond, has_in, inbox, in_key, to):
-        at = lax.rem(owner + lines, lines)
-        box = inbox.at[k, w, at]
-        wait = arrived(box, in_key, k, w, at)
-        out = leaving.at[k, w, at]
-
-        @pl.when(cond)
-        def _():
-            partial[...] = term(k, w, at)
-
-            @pl.when(has_in)
+        return dot(turned[k, w], acts[w, :, cols], 1, 0)
+
+    def route(k, w, t):
+        turn = lax.rem(t // (lines - 1) + z // near, 2)
+        j = lax.rem(t, lines - 1)
+        owner = (1 - turn) * (lines - 1 - j) + turn * j
+        sign = 1 - 2 * turn
+        cond = (owner - z) * sign > 0
+        source = z - sign
+        has_in = jnp.logical_and(source >= 0, source < lines)
+        box = inbox.at[turn, k, w, owner]
+        out = leaving.at[k, w, owner]
+        copy = pltpu.make_async_remote_copy(
+            src_ref=out, dst_ref=box,
+            send_sem=send_sems.at[sent.at("reduce", turn, k, w, owner)],
+            recv_sem=got_sems.at[got.at("reduce", turn, k, w, owner)],
+            device_id=(x, fs + 2 * sign, core), device_id_type=MESH,
+        )
+        return owner, cond, has_in, box, out, copy
+
+    def pieces(k, w):
+        def body(t, carry):
+            owner, cond, has_in, box, out, copy = route(k, w, t)
+
+            @pl.when(cond)
             def _():
-                wait.wait_recv()
-                out[...] = (partial[...] + box[...].astype(jnp.float32)).astype(jnp.bfloat16)
-
-            @pl.when(jnp.logical_not(has_in))
-            def _():
-                out[...] = partial[...].astype(jnp.bfloat16)
-
-        send(out, box, None, to, in_key, k, w, at, cond=cond)
-
-    def reduce_step(k, w, i):
-        reduce_to(k, w, lines - 1 - i, z < lines - 1 - i, has_down, rising, "reduce_up", to_up)
-        reduce_to(k, w, i + 0 * z, z > i, has_up, falling, "reduce_down", to_down)
+                partial[...] = term(k, w, owner)
+
+                @pl.when(has_in)
+                def _():
+                    copy.wait_recv()
+                    out[...] = (partial[...] + box[...].astype(jnp.float32)).astype(jnp.bfloat16)
+
+                @pl.when(jnp.logical_not(has_in))
+                def _():
+                    out[...] = partial[...].astype(jnp.bfloat16)
+
+                copy.start()
+
+            return carry
+
+        lax.fori_loop(0, 2 * (lines - 1), body, 0)
+
+    def pieces_end(k, w):
+        def body(t, carry):
+            _, cond, _, _, _, copy = route(k, w, t)
+            pl.when(cond)(copy.wait_send)
+            return carry
+
+        lax.fori_loop(0, 2 * (lines - 1), body, 0)
+
+    def spread_copies(k, w):
+        here, there, near_ref = spread.at[w, me, k], spread_far.at[k, w], spread.at[w, at_y, k]
+        return (
+            remote(there, here, to_y, "spread_y", k, w),
+            remote(here, here, to_x, "spread_x", k, w, 0),
+            remote(near_ref, near_ref, to_x, "spread_x", k, w, 1),
+        )
 
     def reduce_own(k, w):
         partial[...] = term(k, w, z)
-        for cond, inbox, key in ((has_down, rising, "reduce_up"), (has_up, falling, "reduce_down")):
-            box = inbox.at[k, w, z]
-            wait = arrived(box, key, k, w, z)
+        for turn, cond in ((0, has_down), (1, has_up)):
+            box = inbox.at[turn, k, w, z]
+            wait = arrived(box, "reduce", turn, k, w, z)
 
             @pl.when(cond)
             def _():
                 wait.wait_recv()
                 partial[...] += box[...].astype(jnp.float32)
 
-        here = spread.at[w, me, k]
+        here, there = spread.at[w, me, k], spread_far.at[k, w]
+        there[...] = partial[:, pl.ds(pl.multiple_of((1 - y) * depth, depth), depth)].astype(jnp.bfloat16)
         here[...] = partial[:, pl.ds(pl.multiple_of(y * depth, depth), depth)].astype(jnp.bfloat16)
-        there = spread_far.at[k, w]
-        there[...] = partial[:, pl.ds(pl.multiple_of((1 - y) * depth, depth), depth)].astype(jnp.bfloat16)
-        send(there, here, None, to_y, "spread_y", k, w)
-        send(here, here, None, to_x, "spread_x", k, w, 0)
+        to_near, to_side, _ = spread_copies(k, w)
+        to_near.start()
+        to_side.start()
 
     def spread_relay(k, w):
-        ref = spread.at[w, at_y, k]
-        arrived(ref, "spread_y", k, w).wait_recv()
-        send(ref, ref, None, to_x, "spread_x", k, w, 1)
+        arrived(spread.at[w, at_y, k], "spread_y", k, w).wait_recv()
+        spread_copies(k, w)[2].start()
 
     def spread_wait(k, w):
         arrived(spread.at[w, at_x, k], "spread_x", k, w, 0).wait_recv()
@@ -514,7 +555,7 @@
         for j, (owner, to) in enumerate(((at_far, to_far), (at_x, to_x), (at_y, to_y))):
             for i, part in enumerate(share_term(owner)):
                 share_leaving[j, :, i * wide : (i + 1) * wide] = part.astype(jnp.bfloat16)
-            send(share_leaving.at[j], share_got.at[j], None, to, "share", j)
+            send(share_leaving.at[j], share_got.at[j], to, "share", j)
         for i, part in enumerate(share_term(me)):
             share_sum[:, i * wide : (i + 1) * wide] = part
 
@@ -523,80 +564,102 @@
             arrived(share_got.at[j], "share", j).wait_recv()
             share_sum[...] += share_got[j].astype(jnp.float32)
         place = share_out.at[:, pl.ds(pl.multiple_of(core * mid, mid), mid)]
-        send(share_sum, place, None, to_core, "core_share")
+        send(share_sum, place, to_core, "core_share")
         return fetch(share_sum, place, "share")
 
     pair_send(0)
     for w in range(2):
         gets[0, w].wait()
     line_send(0, y)
-    gets[0].wait()
-    near_send(0)
-    for k in range(1, splits):
-        pair_send(k)
-    gets[1].wait()
-    near_send(1)
+    for t in range(2):
+        gets[t].wait()
+        near_send(t)
     pair_wait(0)
     line_send(0, 1 - y)
     core_up_send(0, z, None)
     for k in range(1, splits):
+        pair_send(k)
         for w in range(2):
             gets[k, w].wait()
-        line_send(k, y)
+        line_send(k, y, end)
     relay(0)
-    gather_step(0, 1, False)
+    gather_step(0, 1)
     for k in range(1, splits):
         pair_wait(k)
-        line_send(k, 1 - y)
+        line_send(k, 1 - y, end)
         core_up_send(k, z, None)
+    for d in range(2, lines - 1):
+        gather_step(0, d)
+    relay(1)
+    for k in range(1, splits):
+        for side in (y, 1 - y):
+            line_send(k, side, middle)
     far_wait(0)
-    relay(1)
-    for d in range(2, lines):
-        gather_step(0, d, False)
+    gather_step(0, lines - 1)
     core_wait(0)
     for i in range(lines):
         forward(0, lax.rem(z + i, lines), i == 0)
+    for k in range(1, splits):
+        gather_step(k, 1, middle)
     far_wait(1)
     core_wait(1)
     for i in range(lines):
         backward(0, lax.rem(z + i, lines), i == 0)
-
-    for k in range(splits):
+    activate(0)
+    for k in range(1, splits):
+        for d in range(2, lines - 1):
+            gather_step(k, d, middle)
+
+    def both_pieces(k):
+        @pl.when(end)
+        def _():
+            for w in range(2):
+                pieces(k, w)
+
+    both_pieces(0)
+    for k in range(1, splits):
+        forward(k, z, True)
+        backward(k, z, True)
+        for d in range(1, lines):
+            gather_step(k, d, end)
+            compute_step(k, d)
         activate(k)
-        last = k == splits - 1
-        if last:
-            share_send()
-        steps = [functools.partial(reduce_step, k, w, i) for w in range(2) for i in range(lines - 1)]
-        steps.insert(lines, functools.partial(reduce_own, k, 0))
-        steps.append(functools.partial(reduce_own, k, 1))
-        fills = []
-        if not last:
-            def begin(k=k):
-                forward(k + 1, z, True)
-                backward(k + 1, z, True)
-
-            fills = [begin] + [functools.partial(gather_step, k + 1, d, True) for d in range(1, lines)]
-        every = max(1, len(steps) // max(1, len(fills)))
-        while steps or fills:
-            for _ in range(every):
-                if steps:
-                    steps.pop(0)()
-            if fills:
-                fills.pop(0)()
-        for w in range(2):
-            spread_relay(k, w)
+        both_pieces(k)
+    share_send()
+
+    grads = [(k, w) for k in range(splits) for w in range(2)]
+
+    @pl.when(middle)
+    def _():
+        for at, (k, w) in enumerate(grads):
+            pieces(k, w)
+            if at:
+                spread_relay(*grads[at - 1])
+            reduce_own(k, w)
+        spread_relay(*grads[-1])
+
+    @pl.when(end)
+    def _():
+        for at, (k, w) in enumerate(grads):
+            reduce_own(k, w)
+            if at:
+                spread_relay(*grads[at - 1])
+        spread_relay(*grads[-1])
 
     out = share_end()
-    for k in range(splits):
-        for w in range(2):
-            spread_wait(k, w)
+    for k, w in grads:
+        spread_wait(k, w)
     ends = [fetch(spread.at[w], ref, "out", w) for w, ref in enumerate((up_out, down_out))]
     arrived(share_out.at[:, pl.ds(pl.multiple_of((1 - core) * mid, mid), mid)], "core_share").wait_recv()
     for cond, copy in pending:
         when(cond, copy.wait_send)
+    for k, w in grads:
+        pieces_end(k, w)
+        for copy in spread_copies(k, w):
+            copy.wait_send()
     out.wait()
-    for end in ends:
-        end.wait()
+    for copy in ends:
+        copy.wait()
 
 
 def plane_fits(inputs, up_weight, down_weight):
@@ -632,8 +695,7 @@
         in_specs=[anywhere] * 4,
         out_specs=(anywhere,) * 3,
         scratch_shapes=[
-            pltpu.VMEM((plane, width), narrow),
-            pltpu.VMEM((plane, width), narrow),
+            pltpu.VMEM((2, plane, width), narrow),
             pltpu.VMEM((splits, lines, wide, step), narrow),
             pltpu.VMEM((splits, lines, step, wide), narrow),
             pltpu.VMEM((splits, lines, wide, step), narrow),
@@ -643,8 +705,7 @@
             pltpu.VMEM((splits, plane, step), narrow),
             pltpu.VMEM((splits, 2, step, plane), narrow),
             pltpu.VMEM((splits, 2, lines, step, wide), narrow),
-            pltpu.VMEM((splits, 2, lines, step, wide), narrow),
-            pltpu.VMEM((splits, 2, lines, step, wide), narrow),
+            pltpu.VMEM((2, splits, 2, lines, step, wide), narrow),
             pltpu.VMEM((step, wide), full),
             pltpu.VMEM((2, 4, splits, step, depth), narrow),
             pltpu.VMEM((splits, 2, step, depth), narrow),

time: 217 us -> 165 us (0.76)
  Pallas kernels: 198 us -> 146 us
  starting transfers between devices: 4.34 us -> 0.96 us
  waiting for transfers between devices: 3.34 us -> 5.76 us
    pallas_call x1, Pallas kernels: 198 us -> 146 us  [plane_plan(): pl.pallas_call(functools.partial(plane_kernel, lines, splits, sent, got,...]
    ppermute x4, starting transfers between devices: 4.34 us -> 0.96 us  [small_sum(): lax.ppermute(value, axis, [(at, at ^ bit) for at in range(size)])]
    ppermute x4, waiting for transfers between devices: 3.34 us -> 5.76 us  [small_sum(): lax.ppermute(value, axis, [(at, at ^ bit) for at in range(size)])]
  transfers between devices with their start and end apart: 4 -> 4, of which waited for: 1 -> 2; matrix products, arithmetic and copies ran while one was open for 3% -> 4% of each run, Pallas kernels for 0% -> 0%
where the time goes in v2:
time: 165 us; the launch traced here: 164 us
  Pallas kernels  146 us (88%)
  other arithmetic  7.22 us (4%)
  waiting for transfers between devices  5.76 us (3%)
  local copies, waits for them, and re-layouts  3.26 us (2%)
    pallas_call x1, Pallas kernels, plane_plan(): pl.pallas_call(functools.partial(plane_kernel, lines, splits, sent, got,...  146 us
    ppermute x4, waiting for transfers between devices, small_sum(): lax.ppermute(value, axis, [(at, at ^ bit) for at in range(size)])  5.76 us
  transfers between devices with their start and end apart: 4, of which 2 were waited for; matrix products, arithmetic and copies ran while one was open for 4% of the time, Pallas kernels for 0%

profile of v2, /device:TPU:0, one launch (start us, length us, event | category | flops | bytes accessed | tf_op | source)
XLA Modules:
  0.0 164.4 jit_solution(10826201201425393244)
XLA Ops:
  0.6 146.5 %plane.1 = (f32[256,2048]{1,0:T(8,128)}, bf16[4,2,256,256]{3,2,1,0:T(8,128)(2,1)}, bf16[4,2,256,256]{3,2,1,0:T(8,128)(2,1)}) custom-call(bf16[256,2048]{1,0:T(8,128)(2,1)} %tokens_hbm.1, bf16[256,2048]{1,0:T(8,128)(2,1)} %cot_hbm.1, bf16[256,2048]{1,0:T(8,128)(2,1)} %up_hbm.1, bf16[2048,256]{1,0:T(8,128)(2,1)} %down_hbm.1), custom_call_target="tpu_custom_call" | custom-call | tf_op jit(solution)/shard_map/plane/pallas_call | solution.py:688
  147.1 1.6 multiply_reduce_fusion
  148.7 0.8 collective-permute-start.1
  149.5 2.7 %bitcast_convert_fusion = f32[2048,256]{1,0:T(8,128)} fusion(bf16[4,2,256,256]{3,2,1,0:T(8,128)(2,1)} %get-tuple-element.9), kind=kLoop, calls=%fused_computation.2 | loop fusion | flops 524288 | bytes 3145728 | tf_op jit(solution)/shard_map/convert_element_type | solution.py:724
  152.2 1.9 %copy.9 = f32[2048,256]{0,1:T(8,128)S(1)} copy(f32[2048,256]{1,0:T(8,128)} %bitcast_convert_fusion) | data formatting | bytes 4194304 | tf_op jit(solution)/shard_map/convert_element_type | solution.py:724
  154.2 0.0 copy-start
  154.2 0.0 copy-start.1
  154.2 0.0 collective-permute-done.1
  154.2 0.1 collective-permute-start.2
  154.3 0.2 multiply_reduce_fusion.1
  154.5 0.0 copy-start.2
  154.5 0.1 collective-permute-start
  154.6 3.3 %collective-permute-done.2 = f32[2048]{0:T(1024)S(1)} collective-permute-done((f32[2048]{0:T(1024)S(1)}, f32[2048]{0:T(1024)S(1)}, u32[]{:S(2)}, u32[]{:S(2)}) %collective-permute-start.2) | collective-permute-done | bytes 8224 | tf_op jit(solution)/shard_map/ppermute | solution.py:95
  157.9 0.0 collective-permute-start.3
  157.9 0.0 copy-done.1
  157.9 1.5 bitcast_convert_fusion.1
  159.5 0.0 copy-done
  159.5 0.0 collective-permute-done
  159.5 0.6 add.12
  160.1 2.4 %collective-permute-done.3 = f32[2048]{0:T(1024)S(1)} collective-permute-done((f32[2048]{0:T(1024)S(1)}, f32[2048]{0:T(1024)S(1)}, u32[]{:S(2)}, u32[]{:S(2)}) %collective-permute-start.3) | collective-permute-done | bytes 8224 | tf_op jit(solution)/shard_map/ppermute | solution.py:95
  162.5 0.6 add.15
  163.1 0.0 copy-done.2
  163.1 1.3 copy.12
  (3 shorter events, 0.0 us)
Async XLA Ops:
  148.7 5.5 %collective-permute-start.1 = (f32[2048]{0:T(1024)S(1)}, f32[2048]{0:T(1024)S(1)}, u32[]{:S(2)}, u32[]{:S(2)}) collective-permute-start(f32[2048]{0:T(1024)S(1)} %bitcast.12), channel_id=1, source_target_pairs={{0,2},{2,0},{4,6},{6,4},{8,10},{10,8},{12,14},{14,12},{1,3},{3,1},... | collective-permute-start | bytes 24584 | tf_op jit(solution)/shard_map/ppermute | solution.py:95
  154.2 5.3 %copy-start = (f32[2048,256]{0,1:T(8,128)}, f32[2048,256]{0,1:T(8,128)S(1)}, u32[]{:S(2)}) copy-start(f32[2048,256]{0,1:T(8,128)S(1)} %copy.9) | copy-start | bytes 6291460
  154.2 3.8 %copy-start.1 = (bf16[4,2,256,256]{3,2,1,0:T(8,128)(2,1)S(1)}, bf16[4,2,256,256]{3,2,1,0:T(8,128)(2,1)}, u32[]{:S(2)}) copy-start(bf16[4,2,256,256]{3,2,1,0:T(8,128)(2,1)} %get-tuple-element.10) | copy-start | bytes 3145732
  154.2 3.7 %collective-permute-start.2 = (f32[2048]{0:T(1024)S(1)}, f32[2048]{0:T(1024)S(1)}, u32[]{:S(2)}, u32[]{:S(2)}) collective-permute-start(f32[2048]{0:T(1024)S(1)} %add.13), channel_id=1, source_target_pairs={{0,4},{2,6},{4,0},{6,2},{8,12},{10,14},{12,8},{14,10},{1,5},{3,7},... | collective-permute-start | bytes 24584 | tf_op jit(solution)/shard_map/ppermute | solution.py:95
  154.5 8.6 %copy-start.2 = (f32[256,2048]{1,0:T(8,128)S(1)}, f32[256,2048]{1,0:T(8,128)}, u32[]{:S(2)}) copy-start(f32[256,2048]{1,0:T(8,128)} %get-tuple-element.16) | copy-start | bytes 6291460
  154.5 5.0 %collective-permute-start = (f32[256]{0:T(256)S(1)}, f32[256]{0:T(256)S(1)}, u32[]{:S(2)}, u32[]{:S(2)}) collective-permute-start(f32[256]{0:T(256)S(1)} %multiply_reduce_fusion.1), channel_id=1, source_target_pairs={{0,1},{1,0},{2,3},{3,2},{4,5},{5,4},{6,7},{7,6},{8,9},{9,8},{10,11... | collective-permute-start | bytes 3080 | tf_op jit(solution)/shard_map/ppermute | solution.py:95
  157.9 4.5 %collective-permute-start.3 = (f32[2048]{0:T(1024)S(1)}, f32[2048]{0:T(1024)S(1)}, u32[]{:S(2)}, u32[]{:S(2)}) collective-permute-start(f32[2048]{0:T(1024)S(1)} %add.14), channel_id=1, source_target_pairs={{0,8},{2,10},{4,12},{6,14},{8,0},{10,2},{12,4},{14,6},{1,9},{3,11}... | collective-permute-start | bytes 24584 | tf_op jit(solution)/shard_map/ppermute | solution.py:95

commit v3 on v2

--- a/solution.py
+++ b/solution.py
@@ -223,7 +223,10 @@
         table.add("spread_x", splits, 2, 2)
         table.add("share", 3)
         table.add("core_share")
+        table.add("core_norms")
         table.add("reduce", 2, splits, 2, lines)
+    sent.add("norms", 2, 2, lines)
+    got.add("norms", lines, 4)
     sent.add("line_up", splits, 2, 2, lines)
     sent.add("line_down", splits, 2, 2, lines)
     got.add("line", splits, 2, 2, lines)
@@ -237,9 +240,10 @@
 def plane_kernel(
     lines, splits, sent, got, local,
     tokens_hbm, cot_hbm, up_hbm, down_hbm,
-    share_out, up_out, down_out,
+    share_out, up_out, down_out, up_norms, down_norms,
     acts, ups, downs, other_up, pre_act, act_grad, pre_grad, other_pre, turned,
     leaving, inbox, partial, spread, spread_far, share_leaving, share_got, share_sum,
+    row_norms, col_norms,
     send_sems, got_sems, local_sems,
 ):
     rows, width = tokens_hbm.shape
@@ -324,19 +328,17 @@
             for t, src in ((0, tokens_hbm), (1, cot_hbm)):
                 gets[t] = fetch(src, band(t, me, 0, rows), "tokens", t)
 
+    others = [
+        (i, j, d, ((x + i) % 2, (z + d) % lines * 2 + (y + j) % 2, core))
+        for i in range(2)
+        for j in range(2)
+        for d in range(lines)
+        if i or j or d
+    ]
     barrier = pltpu.get_barrier_semaphore()
-    for to in (to_x, to_y, to_far, to_core):
+    for to in [to_core] + [other[-1] for other in others]:
         pl.semaphore_signal(barrier, inc=1, device_id=to, device_id_type=MESH)
-
-    @pl.when(has_up)
-    def _():
-        pl.semaphore_signal(barrier, inc=1, device_id=to_up, device_id_type=MESH)
-
-    @pl.when(has_down)
-    def _():
-        pl.semaphore_signal(barrier, inc=1, device_id=to_down, device_id_type=MESH)
-
-    pl.semaphore_wait(barrier, 4 + has_up.astype(jnp.int32) + has_down.astype(jnp.int32))
+    pl.semaphore_wait(barrier, 1 + len(others))
 
     def pair_send(k):
         for w in range(2):
@@ -518,6 +520,14 @@
                 wait.wait_recv()
                 partial[...] += box[...].astype(jnp.float32)
 
+        if w == 1:
+            square = partial[...] * partial[...]
+            folded = square[:, :128]
+            for at in range(128, wide, 128):
+                folded += square[:, at : at + 128]
+            row_norms[z, me, :, k * step : (k + 1) * step] = jnp.broadcast_to(
+                jnp.sum(folded.T, axis=0, keepdims=True), (8, step)
+            )
         here, there = spread.at[w, me, k], spread_far.at[k, w]
         there[...] = partial[:, pl.ds(pl.multiple_of((1 - y) * depth, depth), depth)].astype(jnp.bfloat16)
         here[...] = partial[:, pl.ds(pl.multiple_of(y * depth, depth), depth)].astype(jnp.bfloat16)
@@ -532,6 +542,43 @@
     def spread_wait(k, w):
         arrived(spread.at[w, at_x, k], "spread_x", k, w, 0).wait_recv()
         arrived(spread.at[w, at_far, k], "spread_x", k, w, 1).wait_recv()
+
+    def norm_copies():
+        ref = row_norms.at[z, me]
+        for i, j, d, to in others:
+            yield pltpu.make_async_remote_copy(
+                src_ref=ref, dst_ref=ref,
+                send_sem=send_sems.at[sent.at("norms", i, j, d)],
+                recv_sem=got_sems.at[got.at("norms", z, me)],
+                device_id=to, device_id_type=MESH,
+            )
+
+    def norms_send():
+        for copy in norm_copies():
+            copy.start()
+
+    def norms_end():
+        for i, j, d, _ in others:
+            line, owner = (z + d) % lines, 2 * ((x + i) % 2) + (y + j) % 2
+            arrived(row_norms.at[line, owner], "norms", line, owner).wait_recv()
+        for owner in range(4):
+            total = row_norms[0, owner, 0:1, :]
+            for line in range(1, lines):
+                total += row_norms[line, owner, 0:1, :]
+            down_norms[:, owner * mine : (owner + 1) * mine] = total
+
+    def col_send():
+        total = jnp.zeros((8, depth), jnp.float32)
+        for owner in range(4):
+            for k in range(splits):
+                block = spread[0, owner, k].astype(jnp.float32)
+                total += jnp.sum((block * block).reshape(step // 8, 8, depth), axis=0)
+        col_norms[0] = jnp.broadcast_to(jnp.sum(total, axis=0, keepdims=True), (8, depth))
+        send(col_norms.at[0], col_norms.at[1], to_core, "core_norms")
+
+    def col_end():
+        arrived(col_norms.at[1], "core_norms").wait_recv()
+        up_norms[...] = col_norms[0, 0:1, :] + col_norms[1, 0:1, :]
 
     def share_term(owner):
         at = pl.ds(pl.multiple_of(owner * rows, rows), rows)
@@ -636,6 +683,7 @@
             if at:
                 spread_relay(*grads[at - 1])
             reduce_own(k, w)
+        norms_send()
         spread_relay(*grads[-1])
 
     @pl.when(end)
@@ -644,15 +692,23 @@
             reduce_own(k, w)
             if at:
                 spread_relay(*grads[at - 1])
+        norms_send()
         spread_relay(*grads[-1])
 
     out = share_end()
-    for k, w in grads:
-        spread_wait(k, w)
+    for k in range(splits):
+        spread_wait(k, 0)
+    col_send()
+    norms_end()
+    for k in range(splits):
+        spread_wait(k, 1)
+    col_end()
     ends = [fetch(spread.at[w], ref, "out", w) for w, ref in enumerate((up_out, down_out))]
     arrived(share_out.at[:, pl.ds(pl.multiple_of((1 - core) * mid, mid), mid)], "core_share").wait_recv()
     for cond, copy in pending:
         when(cond, copy.wait_send)
+    for copy in norm_copies():
+        copy.wait_send()
     for k, w in grads:
         pieces_end(k, w)
         for copy in spread_copies(k, w):
@@ -685,15 +741,17 @@
     sent, got, local = plane_slots(lines, splits)
     narrow, full = jnp.bfloat16, jnp.float32
     anywhere = pl.BlockSpec(memory_space=pl.ANY)
-    share, up, down = pl.pallas_call(
+    share, up, down, norms_up, norms_down = pl.pallas_call(
         functools.partial(plane_kernel, lines, splits, sent, got, local),
         out_shape=(
             jax.ShapeDtypeStruct((rows, width), full),
             jax.ShapeDtypeStruct((4, splits, step, depth), narrow),
             jax.ShapeDtypeStruct((4, splits, step, depth), narrow),
+            jax.ShapeDtypeStruct((1, depth), full),
+            jax.ShapeDtypeStruct((1, units), full),
         ),
         in_specs=[anywhere] * 4,
-        out_specs=(anywhere,) * 3,
+        out_specs=(anywhere,) * 3 + (pl.BlockSpec(memory_space=pltpu.VMEM),) * 2,
         scratch_shapes=[
             pltpu.VMEM((2, plane, width), narrow),
             pltpu.VMEM((splits, lines, wide, step), narrow),
@@ -712,6 +770,8 @@
             pltpu.VMEM((3, rows, width // 2), narrow),
             pltpu.VMEM((3, rows, width // 2), narrow),
             pltpu.VMEM((rows, width // 2), full),
+            pltpu.VMEM((lines, 4, 8, units // 4), full),
+            pltpu.VMEM((2, 8, depth), full),
             pltpu.SemaphoreType.DMA((sent.size,)),
             pltpu.SemaphoreType.DMA((got.size,)),
             pltpu.SemaphoreType.DMA((local.size,)),
@@ -723,9 +783,7 @@
     )(inputs, cotangent, up_weight, down_weight)
     grad_up = up.reshape(units, depth).T.astype(full)
     grad_down = down.reshape(units, depth).astype(full)
-    norms_up = small_sum(jnp.sum(grad_up * grad_up, axis=1), "tp")
-    norms_down = small_sum(jnp.sum(grad_down * grad_down, axis=1), "fs")
-    return (share, grad_up, grad_down, norms_up, norms_down)
+    return (share, grad_up, grad_down, norms_up.reshape(depth), norms_down.reshape(units))
 
 
 def shards(inputs, cotangent, up_weight, down_weight):

time: 165 us -> 160 us (0.970)
  waiting for transfers between devices: 5.76 us -> 0 us
  other arithmetic: 7.22 us -> 3.19 us
  Pallas kernels: 146 us -> 149 us
  local copies, waits for them, and re-layouts: 3.26 us -> 6.12 us
    ppermute x4 -> x0, waiting for transfers between devices: 5.76 us -> none  [small_sum(): lax.ppermute(value, axis, [(at, at ^ bit) for at in range(size)])]
    pallas_call x1, Pallas kernels: 146 us -> 149 us  [plane_plan(): pl.pallas_call(functools.partial(plane_kernel, lines, splits, sent, got,...]
    unnamed x8 -> x7, local copies, waits for them, and re-layouts: 1.34 us -> 4.32 us
    convert_element_type x1 -> x0, other arithmetic: 2.7 us -> none  [plane_plan(): grad_up = up.reshape(units, depth).T.astype(full)]
    reduce_sum x2 -> x0, other arithmetic: 1.8 us -> none  [the longest x1 1.58 us: plane_plan(): norms_down = small_sum(jnp.sum(grad_down * grad_down, axis=1), 'fs')]
  transfers between devices with their start and end apart: 4 -> 0, of which waited for: 2 -> 0; matrix products, arithmetic and copies ran while one was open for 4% -> 0% of each run, Pallas kernels for 0% -> 0%
where the time goes in v3:
time: 160 us; the launch traced here: 159 us
  Pallas kernels  149 us (93%)
  local copies, waits for them, and re-layouts  6.12 us (4%)
  other arithmetic  3.19 us (2%)
    pallas_call x1, Pallas kernels, plane_plan(): pl.pallas_call(functools.partial(plane_kernel, lines, splits, sent, got,...  149 us
    unnamed x7, local copies, waits for them, and re-layouts  4.32 us

profile of v3, /device:TPU:0, one launch (start us, length us, event | category | flops | bytes accessed | tf_op | source)
XLA Modules:
  0.0 159.4 jit_solution(351725443120512663)
XLA Ops:
  0.6 149.5 %plane.1 = (f32[256,2048]{1,0:T(8,128)}, bf16[4,2,256,256]{3,2,1,0:T(8,128)(2,1)}, bf16[4,2,256,256]{3,2,1,0:T(8,128)(2,1)}, f32[1,256]{1,0:T(1,128)}, f32[1,2048]{1,0:T(1,128)}) custom-call(bf16[256,2048]{1,0:T(8,128)(2,1)} %tokens_hbm.1, bf16[256,2048]{1,0:T(8,128)(2,1)} %cot_hbm.1, bf16[256,2048]{1,0:T(8,128)(2,1)} %up_hbm.1, bf16[2048,256]{1,0:T(8,128)(2,1)} %down_hbm.1), custom_call_target="tpu_custom_call" | custom-call | tf_op jit(solution)/shard_map/plane/pallas_call | solution.py:744
  150.1 3.2 %bitcast_convert_fusion = (f32[2048,256]{1,0:T(8,128)}, f32[2048,256]{1,0:T(8,128)S(1)}) fusion(bf16[4,2,256,256]{3,2,1,0:T(8,128)(2,1)} %get-tuple-element.12, bf16[4,2,256,256]{3,2,1,0:T(8,128)(2,1)} %get-tuple-element.11), kind=kLoop, calls=%fused_computation | loop fusion | flops 1048576 | bytes 6291456 | tf_op jit(solution)/shard_map/convert_element_type | solution.py:785
  153.3 1.8 %copy.9 = f32[2048,256]{0,1:T(8,128)} copy(f32[2048,256]{1,0:T(8,128)S(1)} %get-tuple-element.16) | data formatting | bytes 4194304 | tf_op jit(solution)/shard_map/convert_element_type | solution.py:784
  155.1 0.0 copy-start.1
  155.1 0.0 copy-start
  155.1 3.1 %copy.13 = f32[256,2048]{1,0:T(8,128)} copy(f32[256,2048]{1,0:T(8,128)} %get-tuple-element.22) | data formatting | bytes 4194304
  158.3 0.0 copy-done.1
  158.3 0.6 copy.14
  158.8 0.0 copy-done
  158.8 0.6 copy.15
Async XLA Ops:
  155.1 3.2 %copy-start.1 = (f32[1,256]{1,0:T(1,128)S(1)}, f32[1,256]{1,0:T(1,128)}, u32[]{:S(2)}) copy-start(f32[1,256]{1,0:T(1,128)} %get-tuple-element.13) | copy-start | bytes 3076
  155.1 3.7 %copy-start = (f32[1,2048]{1,0:T(1,128)S(1)}, f32[1,2048]{1,0:T(1,128)}, u32[]{:S(2)}) copy-start(f32[1,2048]{1,0:T(1,128)} %get-tuple-element.14) | copy-start | bytes 24580

commit v4 on v3

--- a/solution.py
+++ b/solution.py
@@ -180,7 +180,8 @@
 
 
 MESH = pl.DeviceIdType.MESH
-SPLITS = 2
+SPLITS = 4
+LAG = 2
 
 
 def dot(left, right, left_dim, right_dim):
@@ -241,7 +242,7 @@
     lines, splits, sent, got, local,
     tokens_hbm, cot_hbm, up_hbm, down_hbm,
     share_out, up_out, down_out, up_norms, down_norms,
-    acts, ups, downs, other_up, pre_act, act_grad, pre_grad, other_pre, turned,
+    acts, ups, downs, other_up, pre_grad, other_pre, turned,
     leaving, inbox, partial, spread, spread_far, share_leaving, share_got, share_sum,
     row_norms, col_norms,
     send_sems, got_sems, local_sems,
@@ -252,7 +253,7 @@
     step = mine // splits
     wide = 2 * depth
     half = rows // 2
-    bit = half // 2
+    part = half // 4
     near = lines // 2
     mid = width // 2
 
@@ -318,7 +319,7 @@
         return up_hbm.at[:, at] if w == 0 else down_hbm.at[at, :]
 
     def band(t, owner, first, count):
-        return acts.at[t, pl.ds(pl.multiple_of(owner * rows + first, bit), count), :]
+        return acts.at[t, pl.ds(pl.multiple_of(owner * rows + first, part), count), :]
 
     gets = {}
     for k in range(splits):
@@ -336,22 +337,25 @@
         if i or j or d
     ]
     barrier = pltpu.get_barrier_semaphore()
-    for to in [to_core] + [other[-1] for other in others]:
+    for to in (to_x, to_y, to_core):
         pl.semaphore_signal(barrier, inc=1, device_id=to, device_id_type=MESH)
-    pl.semaphore_wait(barrier, 1 + len(others))
+    for cond, to in ((has_up, to_up), (has_down, to_down)):
+
+        @pl.when(cond)
+        def _():
+            pl.semaphore_signal(barrier, inc=1, device_id=to, device_id_type=MESH)
+
+    pl.semaphore_wait(barrier, 3 + has_up.astype(jnp.int32) + has_down.astype(jnp.int32))
 
     def pair_send(k):
         for w in range(2):
             send(own(w, at_y, k), piece(w, k, z, y), to_y, "pair", k, w)
 
-    def line_send(k, side, who=None):
-        up_cond, down_cond = has_up, has_down
-        if who is not None:
-            up_cond, down_cond = jnp.logical_and(has_up, who), jnp.logical_and(has_down, who)
+    def line_send(k, side):
         for w in range(2):
             ref = piece(w, k, z, side)
-            send(ref, ref, to_up, "line_up", k, w, side, z, cond=up_cond, got_key="line")
-            send(ref, ref, to_down, "line_down", k, w, side, z, cond=down_cond, got_key="line")
+            send(ref, ref, to_up, "line_up", k, w, side, z, cond=has_up, got_key="line")
+            send(ref, ref, to_down, "line_down", k, w, side, z, cond=has_down, got_key="line")
 
     def pair_wait(k):
         for w in range(2):
@@ -359,34 +363,42 @@
 
     first = core * half
 
+    cuts = ((0, part), (part, half - part))
+
+    def cut(t, owner, p):
+        return band(t, owner, first + cuts[p][0], cuts[p][1])
+
     def near_send(t):
         for p in range(2):
-            ref = band(t, me, first + p * bit, bit)
+            ref = cut(t, me, p)
             send(ref, ref, to_x, "near_x", t, p)
-            ref = band(t, me, first + (1 - p) * bit, bit)
+            ref = cut(t, me, 1 - p)
             send(ref, ref, to_y, "near_y", t, 1 - p)
 
     def relay(t):
-        ref = band(t, at_x, first, bit)
+        ref = cut(t, at_x, 0)
         arrived(ref, "near_x", t, 0).wait_recv()
         send(ref, ref, to_y, "far", t, 0)
-        ref = band(t, at_y, first + bit, bit)
+        ref = cut(t, at_y, 1)
         arrived(ref, "near_y", t, 1).wait_recv()
         send(ref, ref, to_x, "far", t, 1)
-        arrived(band(t, at_x, first + bit, bit), "near_x", t, 1).wait_recv()
-        arrived(band(t, at_y, first, bit), "near_y", t, 0).wait_recv()
+
+    def near_wait(t):
+        arrived(cut(t, at_x, 1), "near_x", t, 1).wait_recv()
+        arrived(cut(t, at_y, 0), "near_y", t, 0).wait_recv()
         for i, owner in enumerate((at_x, at_y)):
             ref = band(t, owner, first, half)
             send(ref, ref, to_core, "core_tokens", t, i)
 
     def far_wait(t):
         for p in range(2):
-            arrived(band(t, at_far, first + p * bit, bit), "far", t, p).wait_recv()
+            arrived(cut(t, at_far, p), "far", t, p).wait_recv()
         ref = band(t, at_far, first, half)
         send(ref, ref, to_core, "core_tokens", t, 2)
 
-    def core_wait(t):
-        for i, owner in enumerate((at_x, at_y, at_far)):
+    def core_wait(t, *which):
+        for i in which:
+            owner = (at_x, at_y, at_far)[i]
             arrived(band(t, owner, (1 - core) * half, half), "core_tokens", t, i).wait_recv()
 
     def core_up_send(k, line, cond):
@@ -408,7 +420,7 @@
             if who is not None:
                 cond = jnp.logical_and(cond, who)
             for w in range(2):
-                for side in range(2):
+                for side in (y, 1 - y):
                     ref = piece(w, k, line, side)
                     when(cond, arrived(ref, "line", k, w, side, line).wait_recv)
                     send(
@@ -417,35 +429,27 @@
                     )
             core_up_send(k, line, cond)
 
-    def forward(k, line, fresh):
-        cols = pl.ds(pl.multiple_of(line * wide, wide), wide)
-        a = dot(acts[0, :, cols], ups[k, line], 1, 0)
-        pre_act[...] = a if fresh else pre_act[...] + a
-
-    def backward(k, line, fresh):
-        cols = pl.ds(pl.multiple_of(line * wide, wide), wide)
-        a = dot(acts[1, :, cols], downs[k, line], 1, 1)
-        act_grad[...] = a if fresh else act_grad[...] + a
-
-    def compute_step(k, d):
-        for line, cond, _, _, _ in beside(d):
-
-            @pl.when(cond)
-            def _():
-                forward(k, line, False)
-                backward(k, line, False)
-
-    def activate(k):
-        def body(i, carry):
-            at = pl.ds(pl.multiple_of(i * rows, rows), rows)
-            r = jnp.maximum(pre_act[at, :], 0.0)
-            g = (2.0 * r * act_grad[at, :]).astype(jnp.bfloat16)
-            pre_grad[k, at, :] = g
-            turned[k, 0, :, at] = g.T
-            turned[k, 1, :, at] = (r * r).astype(jnp.bfloat16).T
+    def compute(k, owner):
+        at = pl.ds(pl.multiple_of(owner * rows, rows), rows)
+        pre_act = dot(acts[0, at, :], ups[k].reshape(width, step), 1, 0)
+        act_grad = dot(acts[1, at, :wide], downs[k, 0], 1, 1)
+        for line in range(1, lines):
+            act_grad += dot(acts[1, at, line * wide : (line + 1) * wide], downs[k, line], 1, 1)
+        r = jnp.maximum(pre_act, 0.0)
+        g = (2.0 * r * act_grad).astype(jnp.bfloat16)
+        pre_grad[k, at, :] = g
+        turned[k, 0, :, at] = g.T
+        turned[k, 1, :, at] = (r * r).astype(jnp.bfloat16).T
+
+    def compute_all(k):
+        def body(owner, carry):
+            compute(k, owner)
             return carry
 
         lax.fori_loop(0, 4, body, 0)
+        hand_over(k)
+
+    def hand_over(k):
         send(pre_grad.at[k], other_pre.at[k], to_core, "core_pre", k)
 
     def term(k, w, owner):
@@ -470,7 +474,7 @@
         )
         return owner, cond, has_in, box, out, copy
 
-    def pieces(k, w):
+    def pieces(k, w, turn):
         def body(t, carry):
             owner, cond, has_in, box, out, copy = route(k, w, t)
 
@@ -491,7 +495,7 @@
 
             return carry
 
-        lax.fori_loop(0, 2 * (lines - 1), body, 0)
+        lax.fori_loop(turn * (lines - 1), (turn + 1) * (lines - 1), body, 0)
 
     def pieces_end(k, w):
         def body(t, carry):
@@ -614,88 +618,119 @@
         send(share_sum, place, to_core, "core_share")
         return fetch(share_sum, place, "share")
 
-    pair_send(0)
-    for w in range(2):
-        gets[0, w].wait()
-    line_send(0, y)
-    for t in range(2):
-        gets[t].wait()
-        near_send(t)
-    pair_wait(0)
-    line_send(0, 1 - y)
-    core_up_send(0, z, None)
-    for k in range(1, splits):
-        pair_send(k)
+    def line_own(k, side):
+        if side is not y:
+            pair_wait(k)
+        line_send(k, side)
+        if side is not y:
+            core_up_send(k, z, None)
+
+    def gets_wait(k):
         for w in range(2):
             gets[k, w].wait()
-        line_send(k, y, end)
+
+    def finish(at):
+        pieces(*grads[at], 1)
+        if at:
+            spread_relay(*grads[at - 1])
+        reduce_own(*grads[at])
+
+    other = 1 - y
+    pair_send(0)
+    gets_wait(0)
+    line_own(0, y)
+    gets[0].wait()
+    near_send(0)
+    if splits > 1:
+        pair_send(1)
+    gets[1].wait()
+    near_send(1)
+    for k in range(2, splits):
+        pair_send(k)
+    line_own(0, other)
+    if splits > 1:
+        gets_wait(1)
+        line_own(1, y)
     relay(0)
     gather_step(0, 1)
-    for k in range(1, splits):
-        pair_wait(k)
-        line_send(k, 1 - y, end)
-        core_up_send(k, z, None)
+    near_wait(0)
     for d in range(2, lines - 1):
         gather_step(0, d)
+    if splits > 1:
+        line_own(1, other)
+        gather_step(1, 1, middle)
     relay(1)
-    for k in range(1, splits):
-        for side in (y, 1 - y):
-            line_send(k, side, middle)
+    for k in range(2, splits):
+        gets_wait(k)
+        line_own(k, y)
+    near_wait(1)
+    gather_step(0, lines - 1)
+    core_wait(0, 0, 1)
+    core_wait(1, 0, 1)
+    if splits > 1:
+        for d in range(2, lines - 1):
+            gather_step(1, d, middle)
+    for owner in (me, at_x, at_y):
+        compute(0, owner)
+    for k in range(2, splits):
+        line_own(k, other)
     far_wait(0)
-    gather_step(0, lines - 1)
-    core_wait(0)
-    for i in range(lines):
-        forward(0, lax.rem(z + i, lines), i == 0)
-    for k in range(1, splits):
-        gather_step(k, 1, middle)
     far_wait(1)
-    core_wait(1)
-    for i in range(lines):
-        backward(0, lax.rem(z + i, lines), i == 0)
-    activate(0)
-    for k in range(1, splits):
-        for d in range(2, lines - 1):
-            gather_step(k, d, middle)
+    core_wait(0, 2)
+    core_wait(1, 2)
+    compute(0, at_far)
+    hand_over(0)
+
+    grads = [(k, w) for k in range(splits) for w in range(2)]
+    jobs = []
+    for at, (k, w) in enumerate(grads):
+        jobs.append(functools.partial(pieces, k, w, 0))
+        if at >= LAG:
+            jobs.append(functools.partial(finish, at - LAG))
+    jobs += [functools.partial(finish, at) for at in range(max(0, len(grads) - LAG), len(grads) - 1)]
+    jobs.append(functools.partial(pieces, *grads[-1], 1))
 
     def both_pieces(k):
         @pl.when(end)
         def _():
             for w in range(2):
-                pieces(k, w)
+                pieces(k, w, 0)
+
+        if k >= splits - 2 and k:
+
+            @pl.when(middle)
+            def _():
+                jobs.pop(0)()
 
     both_pieces(0)
     for k in range(1, splits):
-        forward(k, z, True)
-        backward(k, z, True)
+        if k + 1 < splits:
+            for d in range(1, lines - 1):
+                gather_step(k + 1, d, middle)
         for d in range(1, lines):
             gather_step(k, d, end)
-            compute_step(k, d)
-        activate(k)
+        compute_all(k)
         both_pieces(k)
     share_send()
 
-    grads = [(k, w) for k in range(splits) for w in range(2)]
-
     @pl.when(middle)
     def _():
-        for at, (k, w) in enumerate(grads):
-            pieces(k, w)
-            if at:
-                spread_relay(*grads[at - 1])
-            reduce_own(k, w)
-        norms_send()
-        spread_relay(*grads[-1])
+        while jobs:
+            jobs.pop(0)()
 
     @pl.when(end)
     def _():
-        for at, (k, w) in enumerate(grads):
+        for at, (k, w) in enumerate(grads[:-1]):
             reduce_own(k, w)
             if at:
                 spread_relay(*grads[at - 1])
-        norms_send()
-        spread_relay(*grads[-1])
 
     out = share_end()
+    if len(grads) > 1:
+        spread_relay(*grads[-2])
+    reduce_own(*grads[-1])
+    norms_send()
+    spread_relay(*grads[-1])
     for k in range(splits):
         spread_wait(k, 0)
     col_send()
@@ -725,7 +760,7 @@
     rows, width = inputs.shape
     depth, units = up_weight.shape
     step = units // 4 // SPLITS
-    even = rows % 64 == 0 and depth % 128 == 0 and step % 128 == 0 and width == groups * depth
+    even = rows % 128 == 0 and depth % 128 == 0 and step % 128 == 0 and width == groups * depth
     held = 2 * 4 * rows * width * 2 + 4 * (units // 4) * width * 2
     return even and held <= 16 * 2**20
 
@@ -757,8 +792,6 @@
             pltpu.VMEM((splits, lines, wide, step), narrow),
             pltpu.VMEM((splits, lines, step, wide), narrow),
             pltpu.VMEM((splits, lines, wide, step), narrow),
-            pltpu.VMEM((plane, step), full),
-            pltpu.VMEM((plane, step), full),
             pltpu.VMEM((splits, plane, step), narrow),
             pltpu.VMEM((splits, plane, step), narrow),
             pltpu.VMEM((splits, 2, step, plane), narrow),

time: 160 us -> 154 us (0.963)
  Pallas kernels: 149 us -> 144 us
    pallas_call x1, Pallas kernels: 149 us -> 144 us  [plane_plan(): pl.pallas_call(functools.partial(plane_kernel, lines, splits, sent, got,...]
where the time goes in v4:
time: 154 us
  Pallas kernels  144 us (94%)
  local copies, waits for them, and re-layouts  6.12 us (4%)
  other arithmetic  3.19 us (2%)
    pallas_call x1, Pallas kernels, plane_plan(): pl.pallas_call(functools.partial(plane_kernel, lines, splits, sent, got,...  144 us
    unnamed x7, local copies, waits for them, and re-layouts  4.32 us
    convert_element_type x1, other arithmetic, plane_plan(): grad_down = down.reshape(units, depth).astype(full)  3.19 us

profile of v4, /device:TPU:0, one launch (start us, length us, event | category | flops | bytes accessed | tf_op | source)
XLA Modules:
  0.0 153.6 jit_solution(11453508424779147684)
XLA Ops:
  0.6 143.6 %plane.1 = (f32[256,2048]{1,0:T(8,128)}, bf16[4,4,128,256]{3,2,1,0:T(8,128)(2,1)}, bf16[4,4,128,256]{3,2,1,0:T(8,128)(2,1)}, f32[1,256]{1,0:T(1,128)}, f32[1,2048]{1,0:T(1,128)}) custom-call(bf16[256,2048]{1,0:T(8,128)(2,1)} %tokens_hbm.1, bf16[256,2048]{1,0:T(8,128)(2,1)} %cot_hbm.1, bf16[256,2048]{1,0:T(8,128)(2,1)} %up_hbm.1, bf16[2048,256]{1,0:T(8,128)(2,1)} %down_hbm.1), custom_call_target="tpu_custom_call" | custom-call | tf_op jit(solution)/shard_map/plane/pallas_call | solution.py:779
  144.3 3.2 %bitcast_convert_fusion = (f32[2048,256]{1,0:T(8,128)}, f32[2048,256]{1,0:T(8,128)S(1)}) fusion(bf16[4,4,128,256]{3,2,1,0:T(8,128)(2,1)} %get-tuple-element.12, bf16[4,4,128,256]{3,2,1,0:T(8,128)(2,1)} %get-tuple-element.11), kind=kLoop, calls=%fused_computation | loop fusion | flops 1048576 | bytes 6291456 | tf_op jit(solution)/shard_map/convert_element_type | solution.py:818
  147.5 1.8 %copy.9 = f32[2048,256]{0,1:T(8,128)} copy(f32[2048,256]{1,0:T(8,128)S(1)} %get-tuple-element.16) | data formatting | bytes 4194304 | tf_op jit(solution)/shard_map/convert_element_type | solution.py:817
  149.3 0.0 copy-start.1
  149.3 0.0 copy-start
  149.3 3.1 %copy.13 = f32[256,2048]{1,0:T(8,128)} copy(f32[256,2048]{1,0:T(8,128)} %get-tuple-element.22) | data formatting | bytes 4194304
  152.4 0.0 copy-done.1
  152.4 0.6 copy.14
  153.0 0.0 copy-done
  153.0 0.6 copy.15
Async XLA Ops:
  149.3 3.2 %copy-start.1 = (f32[1,256]{1,0:T(1,128)S(1)}, f32[1,256]{1,0:T(1,128)}, u32[]{:S(2)}) copy-start(f32[1,256]{1,0:T(1,128)} %get-tuple-element.13) | copy-start | bytes 3076
  149.3 3.7 %copy-start = (f32[1,2048]{1,0:T(1,128)S(1)}, f32[1,2048]{1,0:T(1,128)}, u32[]{:S(2)}) copy-start(f32[1,2048]{1,0:T(1,128)} %get-tuple-element.14) | copy-start | bytes 24580

commit v5 on v4

--- a/solution.py
+++ b/solution.py
@@ -181,7 +181,6 @@
 
 MESH = pl.DeviceIdType.MESH
 SPLITS = 4
-LAG = 2
 
 
 def dot(left, right, left_dim, right_dim):
@@ -224,6 +223,7 @@
         table.add("spread_x", splits, 2, 2)
         table.add("share", 3)
         table.add("core_share")
+        table.add("core_extra")
         table.add("core_norms")
         table.add("reduce", 2, splits, 2, lines)
     sent.add("norms", 2, 2, lines)
@@ -233,18 +233,20 @@
     got.add("line", splits, 2, 2, lines)
     local.add("tokens", 2)
     local.add("weights", splits, 2)
-    local.add("share")
-    local.add("out", 2)
+    local.add("core_share")
+    local.add("core_extra")
+    local.add("up", splits, 4)
+    local.add("down", splits)
     return sent, got, local
 
 
 def plane_kernel(
     lines, splits, sent, got, local,
     tokens_hbm, cot_hbm, up_hbm, down_hbm,
-    share_out, up_out, down_out, up_norms, down_norms,
+    share_out, extra_out, up_out, down_out, up_norms, down_norms,
     acts, ups, downs, other_up, pre_grad, other_pre, turned,
     leaving, inbox, partial, spread, spread_far, share_leaving, share_got, share_sum,
-    row_norms, col_norms,
+    row_norms, col_norms, up_turned,
     send_sems, got_sems, local_sems,
 ):
     rows, width = tokens_hbm.shape
@@ -474,8 +476,10 @@
         )
         return owner, cond, has_in, box, out, copy
 
-    def pieces(k, w, turn):
-        def body(t, carry):
+    def pieces(k, turn):
+        def body(u, carry):
+            w = lax.rem(u, 2)
+            t = turn * (lines - 1) + u // 2
             owner, cond, has_in, box, out, copy = route(k, w, t)
 
             @pl.when(cond)
@@ -495,7 +499,7 @@
 
             return carry
 
-        lax.fori_loop(turn * (lines - 1), (turn + 1) * (lines - 1), body, 0)
+        lax.fori_loop(0, 2 * (lines - 1), body, 0)
 
     def pieces_end(k, w):
         def body(t, carry):
@@ -571,14 +575,25 @@
                 total += row_norms[line, owner, 0:1, :]
             down_norms[:, owner * mine : (owner + 1) * mine] = total
 
-    def col_send():
-        total = jnp.zeros((8, depth), jnp.float32)
+    def deliver(k):
+        spread_wait(k, 0)
+        total = jnp.zeros((8, depth), jnp.float32) if k == 0 else col_norms[0]
+        copies = []
         for owner in range(4):
-            for k in range(splits):
-                block = spread[0, owner, k].astype(jnp.float32)
-                total += jnp.sum((block * block).reshape(step // 8, 8, depth), axis=0)
-        col_norms[0] = jnp.broadcast_to(jnp.sum(total, axis=0, keepdims=True), (8, depth))
-        send(col_norms.at[0], col_norms.at[1], to_core, "core_norms")
+            block = spread[0, owner, k]
+            wider = block.astype(jnp.float32)
+            total += jnp.sum((wider * wider).reshape(step // 8, 8, depth), axis=0)
+            at = pl.ds(owner * mine + k * step, step)
+            up_turned[:, at] = block.T
+            copies.append(fetch(up_turned.at[:, at], up_out.at[:, at], "up", k, owner))
+        if k == splits - 1:
+            total = jnp.broadcast_to(jnp.sum(total, axis=0, keepdims=True), (8, depth))
+        col_norms[0] = total
+        if k == splits - 1:
+            send(col_norms.at[0], col_norms.at[1], to_core, "core_norms")
+        spread_wait(k, 1)
+        copies.append(fetch(spread.at[1, :, k], down_out.at[:, k], "down", k))
+        return copies
 
     def col_end():
         arrived(col_norms.at[1], "core_norms").wait_recv()
@@ -610,13 +625,19 @@
         for i, part in enumerate(share_term(me)):
             share_sum[:, i * wide : (i + 1) * wide] = part
 
+    share_keys = ("core_share", "core_extra")
+
     def share_end():
         for j in range(3):
             arrived(share_got.at[j], "share", j).wait_recv()
-            share_sum[...] += share_got[j].astype(jnp.float32)
-        place = share_out.at[:, pl.ds(pl.multiple_of(core * mid, mid), mid)]
-        send(share_sum, place, to_core, "core_share")
-        return fetch(share_sum, place, "share")
+            if j:
+                share_sum[...] += share_got[j].astype(jnp.float32)
+        copies = []
+        for src, ref, key in zip((share_sum, share_got.at[0]), (share_out, extra_out), share_keys, strict=True):
+            place = ref.at[:, pl.ds(pl.multiple_of(core * mid, mid), mid)]
+            send(src, place, to_core, key)
+            copies.append(fetch(src, place, key))
+        return copies
 
     def line_own(k, side):
         if side is not y:
@@ -629,11 +650,15 @@
         for w in range(2):
             gets[k, w].wait()
 
-    def finish(at):
-        pieces(*grads[at], 1)
-        if at:
-            spread_relay(*grads[at - 1])
-        reduce_own(*grads[at])
+    def own_pair(k):
+        for w in range(2):
+            if k:
+                spread_relay(k - 1, w)
+            reduce_own(k, w)
+
+    def finish(k):
+        pieces(k, 1)
+        own_pair(k)
 
     other = 1 - y
     pair_send(0)
@@ -683,24 +708,16 @@
 
     grads = [(k, w) for k in range(splits) for w in range(2)]
     jobs = []
-    for at, (k, w) in enumerate(grads):
-        jobs.append(functools.partial(pieces, k, w, 0))
-        if at >= LAG:
-            jobs.append(functools.partial(finish, at - LAG))
-    jobs += [functools.partial(finish, at) for at in range(max(0, len(grads) - LAG), len(grads) - 1)]
-    jobs.append(functools.partial(pieces, *grads[-1], 1))
+    for k in range(splits):
+        jobs.append(functools.partial(pieces, k, 0))
+        if k:
+            jobs.append(functools.partial(finish, k - 1))
+    jobs.append(functools.partial(pieces, splits - 1, 1))
 
     def both_pieces(k):
         @pl.when(end)
         def _():
-            for w in range(2):
-                pieces(k, w, 0)
-
-        if k >= splits - 2 and k:
-
-            @pl.when(middle)
-            def _():
-                jobs.pop(0)()
+            pieces(k, 0)
 
     both_pieces(0)
     for k in range(1, splits):
@@ -715,31 +732,28 @@
 
     @pl.when(middle)
     def _():
-        while jobs:
-            jobs.pop(0)()
+        for job in jobs:
+            job()
 
     @pl.when(end)
     def _():
-        for at, (k, w) in enumerate(grads[:-1]):
-            reduce_own(k, w)
-            if at:
-                spread_relay(*grads[at - 1])
-
-    out = share_end()
-    if len(grads) > 1:
-        spread_relay(*grads[-2])
-    reduce_own(*grads[-1])
+        for k in range(splits - 1):
+            own_pair(k)
+
+    ends = share_end()
+    for k in range(splits - 2):
+        ends += deliver(k)
+    own_pair(splits - 1)
     norms_send()
-    spread_relay(*grads[-1])
-    for k in range(splits):
-        spread_wait(k, 0)
-    col_send()
+    if splits > 1:
+        ends += deliver(splits - 2)
+    for w in range(2):
+        spread_relay(splits - 1, w)
     norms_end()
-    for k in range(splits):
-        spread_wait(k, 1)
+    ends += deliver(splits - 1)
     col_end()
-    ends = [fetch(spread.at[w], ref, "out", w) for w, ref in enumerate((up_out, down_out))]
-    arrived(share_out.at[:, pl.ds(pl.multiple_of((1 - core) * mid, mid), mid)], "core_share").wait_recv()
+    for ref in (share_out, extra_out):
+        arrived(ref.at[:, pl.ds(pl.multiple_of((1 - core) * mid, mid), mid)], share_keys[ref is extra_out]).wait_recv()
     for cond, copy in pending:
         when(cond, copy.wait_send)
     for copy in norm_copies():
@@ -748,7 +762,6 @@
         pieces_end(k, w)
         for copy in spread_copies(k, w):
             copy.wait_send()
-    out.wait()
     for copy in ends:
         copy.wait()
 
@@ -776,17 +789,18 @@
     sent, got, local = plane_slots(lines, splits)
     narrow, full = jnp.bfloat16, jnp.float32
     anywhere = pl.BlockSpec(memory_space=pl.ANY)
-    share, up, down, norms_up, norms_down = pl.pallas_call(
+    share, extra, up, down, norms_up, norms_down = pl.pallas_call(
         functools.partial(plane_kernel, lines, splits, sent, got, local),
         out_shape=(
             jax.ShapeDtypeStruct((rows, width), full),
-            jax.ShapeDtypeStruct((4, splits, step, depth), narrow),
+            jax.ShapeDtypeStruct((rows, width), narrow),
+            jax.ShapeDtypeStruct((depth, units), narrow),
             jax.ShapeDtypeStruct((4, splits, step, depth), narrow),
             jax.ShapeDtypeStruct((1, depth), full),
             jax.ShapeDtypeStruct((1, units), full),
         ),
         in_specs=[anywhere] * 4,
-        out_specs=(anywhere,) * 3 + (pl.BlockSpec(memory_space=pltpu.VMEM),) * 2,
+        out_specs=(anywhere,) * 4 + (pl.BlockSpec(memory_space=pltpu.VMEM),) * 2,
         scratch_shapes=[
             pltpu.VMEM((2, plane, width), narrow),
             pltpu.VMEM((splits, lines, wide, step), narrow),
@@ -805,6 +819,7 @@
             pltpu.VMEM((rows, width // 2), full),
             pltpu.VMEM((lines, 4, 8, units // 4), full),
             pltpu.VMEM((2, 8, depth), full),
+            pltpu.VMEM((depth, units), narrow),
             pltpu.SemaphoreType.DMA((sent.size,)),
             pltpu.SemaphoreType.DMA((got.size,)),
             pltpu.SemaphoreType.DMA((local.size,)),
@@ -814,7 +829,8 @@
         ),
         name="plane",
     )(inputs, cotangent, up_weight, down_weight)
-    grad_up = up.reshape(units, depth).T.astype(full)
+    grad_up = up.astype(full)
+    share = share + extra.astype(full)
     grad_down = down.reshape(units, depth).astype(full)
     return (share, grad_up, grad_down, norms_up.reshape(depth), norms_down.reshape(units))
 

time: 154 us -> 150 us (0.974)
  local copies, waits for them, and re-layouts: 6.12 us -> 1.18 us
  other arithmetic: 3.19 us -> 6.73 us
  Pallas kernels: 144 us -> 141 us
    add x0 -> x1, other arithmetic: none -> 3.63 us  [plane_plan(): share = share + extra.astype(full)]
    unnamed x7 -> x10, local copies, waits for them, and re-layouts: 4.32 us -> 1.18 us
    pallas_call x1, Pallas kernels: 144 us -> 141 us  [plane_plan(): pl.pallas_call(functools.partial(plane_kernel, lines, splits, sent, got,...]
    convert_element_type x1 -> x0, local copies, waits for them, and re-layouts: 1.8 us -> none  [plane_plan(): grad_up = up.reshape(units, depth).T.astype(full)]
    convert_element_type x1, other arithmetic: 3.19 us -> 1.55 us  [plane_plan(): grad_down = down.reshape(units, depth).astype(full)]
    convert_element_type x0 -> x1, other arithmetic: none -> 1.55 us  [plane_plan(): grad_up = up.astype(full)]
where the time goes in v5:
time: 150 us; the launch traced here: 149 us
  Pallas kernels  141 us (94%)
  other arithmetic  6.73 us (4%)
    pallas_call x1, Pallas kernels, plane_plan(): pl.pallas_call(functools.partial(plane_kernel, lines, splits, sent, got,...  141 us
    add x1, other arithmetic, plane_plan(): share = share + extra.astype(full)  3.63 us

profile of v5, /device:TPU:0, one launch (start us, length us, event | category | flops | bytes accessed | tf_op | source)
XLA Modules:
  0.0 149.5 jit_solution(844483274170118051)
XLA Ops:
  0.6 140.9 %plane.1 = (f32[256,2048]{1,0:T(8,128)}, bf16[256,2048]{1,0:T(8,128)(2,1)}, bf16[256,2048]{1,0:T(8,128)(2,1)}, bf16[4,4,128,256]{3,2,1,0:T(8,128)(2,1)}, f32[1,256]{1,0:T(1,128)}, /*index=5*/f32[1,2048]{1,0:T(1,128)}) custom-call(bf16[256,2048]{1,0:T(8,128)(2,1)} %tokens_hbm.1, bf16[256,2048]{1,0:T(8,128)(2,1)} %cot_hbm.1, bf16[256,2048]{1,0:T(8,128)(2,1)} %up_hbm.1, ...), custom_call_target="tpu_custom_call" | custom-call | tf_op jit(solution)/shard_map/plane/pallas_call | solution.py:792
  141.5 0.0 copy-start.1
  141.6 3.6 %convert_add_fusion = f32[256,2048]{1,0:T(8,128)} fusion(f32[256,2048]{1,0:T(8,128)} %get-tuple-element.11, bf16[256,2048]{1,0:T(8,128)(2,1)} %get-tuple-element.12), kind=kLoop, calls=%fused_computation | loop fusion | flops 1048576 | bytes 5242880 | tf_op jit(solution)/shard_map/add | solution.py:833
  145.2 0.0 copy-done.1
  145.2 0.0 copy-start
  145.2 1.5 %convert_element_type.13 = f32[256,2048]{1,0:T(8,128)} convert(bf16[256,2048]{1,0:T(8,128)(2,1)S(1)} %copy-done.1) | non-fusion elementwise | flops 524288 | bytes 3145728 | tf_op jit(solution)/shard_map/convert_element_type | solution.py:832
  146.7 0.0 copy-done
  146.7 0.0 copy-start.3
  146.7 0.0 copy-start.2
  146.7 1.5 %bitcast_convert_fusion = f32[2048,256]{1,0:T(8,128)} fusion(bf16[4,4,128,256]{3,2,1,0:T(8,128)(2,1)S(1)} %copy-done), kind=kLoop, calls=%fused_computation.1 | loop fusion | flops 524288 | bytes 3145728 | tf_op jit(solution)/shard_map/convert_element_type | solution.py:834
  148.3 0.0 copy-done.3
  148.3 0.6 copy.11
  148.9 0.0 copy-done.2
  148.9 0.6 copy.12
Async XLA Ops:
  141.5 3.6 %copy-start.1 = (bf16[256,2048]{1,0:T(8,128)(2,1)S(1)}, bf16[256,2048]{1,0:T(8,128)(2,1)}, u32[]{:S(2)}) copy-start(bf16[256,2048]{1,0:T(8,128)(2,1)} %get-tuple-element.13) | copy-start | bytes 3145732
  145.2 1.6 %copy-start = (bf16[4,4,128,256]{3,2,1,0:T(8,128)(2,1)S(1)}, bf16[4,4,128,256]{3,2,1,0:T(8,128)(2,1)}, u32[]{:S(2)}) copy-start(bf16[4,4,128,256]{3,2,1,0:T(8,128)(2,1)} %get-tuple-element.14) | copy-start | bytes 3145732
  146.7 1.6 %copy-start.3 = (f32[1,256]{1,0:T(1,128)S(1)}, f32[1,256]{1,0:T(1,128)}, u32[]{:S(2)}) copy-start(f32[1,256]{1,0:T(1,128)} %get-tuple-element.15) | copy-start | bytes 3076
  146.7 2.1 %copy-start.2 = (f32[1,2048]{1,0:T(1,128)S(1)}, f32[1,2048]{1,0:T(1,128)}, u32[]{:S(2)}) copy-start(f32[1,2048]{1,0:T(1,128)} %get-tuple-element.16) | copy-start | bytes 24580

commit v6 on v5

--- a/solution.py
+++ b/solution.py
@@ -244,7 +244,7 @@
     lines, splits, sent, got, local,
     tokens_hbm, cot_hbm, up_hbm, down_hbm,
     share_out, extra_out, up_out, down_out, up_norms, down_norms,
-    acts, ups, downs, other_up, pre_grad, other_pre, turned,
+    acts, ups, downs, other_up, rectified, pre_grad, other_pre, turned,
     leaving, inbox, partial, spread, spread_far, share_leaving, share_got, share_sum,
     row_norms, col_norms, up_turned,
     send_sems, got_sems, local_sems,
@@ -431,25 +431,31 @@
                     )
             core_up_send(k, line, cond)
 
-    def compute(k, owner):
+    def hidden(k, owner):
         at = pl.ds(pl.multiple_of(owner * rows, rows), rows)
-        pre_act = dot(acts[0, at, :], ups[k].reshape(width, step), 1, 0)
+        r = jnp.maximum(dot(acts[0, at, :], ups[k].reshape(width, step), 1, 0), 0.0)
+        rectified[at, :] = r
+        turned[k, 1, :, at] = (r * r).astype(jnp.bfloat16).T
+
+    def gradient(k, owner):
+        at = pl.ds(pl.multiple_of(owner * rows, rows), rows)
         act_grad = dot(acts[1, at, :wide], downs[k, 0], 1, 1)
         for line in range(1, lines):
             act_grad += dot(acts[1, at, line * wide : (line + 1) * wide], downs[k, line], 1, 1)
-        r = jnp.maximum(pre_act, 0.0)
-        g = (2.0 * r * act_grad).astype(jnp.bfloat16)
+        g = (2.0 * rectified[at, :] * act_grad).astype(jnp.bfloat16)
         pre_grad[k, at, :] = g
         turned[k, 0, :, at] = g.T
-        turned[k, 1, :, at] = (r * r).astype(jnp.bfloat16).T
-
-    def compute_all(k):
+
+    def compute(k, owner):
+        hidden(k, owner)
+        gradient(k, owner)
+
+    def every(act, k):
         def body(owner, carry):
-            compute(k, owner)
+            act(k, owner)
             return carry
 
         lax.fori_loop(0, 4, body, 0)
-        hand_over(k)
 
     def hand_over(k):
         send(pre_grad.at[k], other_pre.at[k], to_core, "core_pre", k)
@@ -478,7 +484,7 @@
 
     def pieces(k, turn):
         def body(u, carry):
-            w = lax.rem(u, 2)
+            w = 1 - lax.rem(u, 2)
             t = turn * (lines - 1) + u // 2
             owner, cond, has_in, box, out, copy = route(k, w, t)
 
@@ -533,9 +539,7 @@
             folded = square[:, :128]
             for at in range(128, wide, 128):
                 folded += square[:, at : at + 128]
-            row_norms[z, me, :, k * step : (k + 1) * step] = jnp.broadcast_to(
-                jnp.sum(folded.T, axis=0, keepdims=True), (8, step)
-            )
+            row_norms[z, me, :, k * step : (k + 1) * step] = jnp.sum(folded.T, axis=0, keepdims=True)
         here, there = spread.at[w, me, k], spread_far.at[k, w]
         there[...] = partial[:, pl.ds(pl.multiple_of((1 - y) * depth, depth), depth)].astype(jnp.bfloat16)
         here[...] = partial[:, pl.ds(pl.multiple_of(y * depth, depth), depth)].astype(jnp.bfloat16)
@@ -576,9 +580,10 @@
             down_norms[:, owner * mine : (owner + 1) * mine] = total
 
     def deliver(k):
+        spread_wait(k, 1)
+        copies = [fetch(spread.at[1, :, k], down_out.at[:, k], "down", k)]
         spread_wait(k, 0)
         total = jnp.zeros((8, depth), jnp.float32) if k == 0 else col_norms[0]
-        copies = []
         for owner in range(4):
             block = spread[0, owner, k]
             wider = block.astype(jnp.float32)
@@ -591,8 +596,6 @@
         col_norms[0] = total
         if k == splits - 1:
             send(col_norms.at[0], col_norms.at[1], to_core, "core_norms")
-        spread_wait(k, 1)
-        copies.append(fetch(spread.at[1, :, k], down_out.at[:, k], "down", k))
         return copies
 
     def col_end():
@@ -651,10 +654,12 @@
             gets[k, w].wait()
 
     def own_pair(k):
-        for w in range(2):
+        for w in (1, 0):
             if k:
                 spread_relay(k - 1, w)
             reduce_own(k, w)
+            if w == 1 and k == splits - 1:
+                norms_send()
 
     def finish(k):
         pieces(k, 1)
@@ -700,10 +705,11 @@
     for k in range(2, splits):
         line_own(k, other)
     far_wait(0)
+    core_wait(0, 2)
+    hidden(0, at_far)
     far_wait(1)
-    core_wait(0, 2)
     core_wait(1, 2)
-    compute(0, at_far)
+    gradient(0, at_far)
     hand_over(0)
 
     grads = [(k, w) for k in range(splits) for w in range(2)]
@@ -714,20 +720,21 @@
             jobs.append(functools.partial(finish, k - 1))
     jobs.append(functools.partial(pieces, splits - 1, 1))
 
-    def both_pieces(k):
+    def end_pieces(k):
         @pl.when(end)
         def _():
             pieces(k, 0)
 
-    both_pieces(0)
+    end_pieces(0)
     for k in range(1, splits):
         if k + 1 < splits:
             for d in range(1, lines - 1):
                 gather_step(k + 1, d, middle)
         for d in range(1, lines):
             gather_step(k, d, end)
-        compute_all(k)
-        both_pieces(k)
+        every(compute, k)
+        hand_over(k)
+        end_pieces(k)
     share_send()
 
     @pl.when(middle)
@@ -744,10 +751,9 @@
     for k in range(splits - 2):
         ends += deliver(k)
     own_pair(splits - 1)
-    norms_send()
     if splits > 1:
         ends += deliver(splits - 2)
-    for w in range(2):
+    for w in (1, 0):
         spread_relay(splits - 1, w)
     norms_end()
     ends += deliver(splits - 1)
@@ -806,6 +812,7 @@
             pltpu.VMEM((splits, lines, wide, step), narrow),
             pltpu.VMEM((splits, lines, step, wide), narrow),
             pltpu.VMEM((splits, lines, wide, step), narrow),
+            pltpu.VMEM((plane, step), full),
             pltpu.VMEM((splits, plane, step), narrow),
             pltpu.VMEM((splits, plane, step), narrow),
             pltpu.VMEM((splits, 2, step, plane), narrow),
@@ -817,7 +824,7 @@
             pltpu.VMEM((3, rows, width // 2), narrow),
             pltpu.VMEM((3, rows, width // 2), narrow),
             pltpu.VMEM((rows, width // 2), full),
-            pltpu.VMEM((lines, 4, 8, units // 4), full),
+            pltpu.VMEM((lines, 4, 1, units // 4), full),
             pltpu.VMEM((2, 8, depth), full),
             pltpu.VMEM((depth, units), narrow),
             pltpu.SemaphoreType.DMA((sent.size,)),

time: 150 us -> 148 us (0.987)
  no operation moved by 1% of the time
where the time goes in v6:
time: 148 us
  Pallas kernels  140 us (95%)
  other arithmetic  6.73 us (5%)
    pallas_call x1, Pallas kernels, plane_plan(): pl.pallas_call(functools.partial(plane_kernel, lines, splits, sent, got,...  140 us
    add x1, other arithmetic, plane_plan(): share = share + extra.astype(full)  3.63 us

profile of v6, /device:TPU:0, one launch (start us, length us, event | category | flops | bytes accessed | tf_op | source)
XLA Modules:
  0.0 148.1 jit_solution(5195104502851270820)
XLA Ops:
  0.6 139.5 %plane.1 = (f32[256,2048]{1,0:T(8,128)}, bf16[256,2048]{1,0:T(8,128)(2,1)}, bf16[256,2048]{1,0:T(8,128)(2,1)}, bf16[4,4,128,256]{3,2,1,0:T(8,128)(2,1)}, f32[1,256]{1,0:T(1,128)}, /*index=5*/f32[1,2048]{1,0:T(1,128)}) custom-call(bf16[256,2048]{1,0:T(8,128)(2,1)} %tokens_hbm.1, bf16[256,2048]{1,0:T(8,128)(2,1)} %cot_hbm.1, bf16[256,2048]{1,0:T(8,128)(2,1)} %up_hbm.1, ...), custom_call_target="tpu_custom_call" | custom-call | tf_op jit(solution)/shard_map/plane/pallas_call | solution.py:798
  140.1 0.0 copy-start.1
  140.2 3.6 %convert_add_fusion = f32[256,2048]{1,0:T(8,128)} fusion(f32[256,2048]{1,0:T(8,128)} %get-tuple-element.11, bf16[256,2048]{1,0:T(8,128)(2,1)} %get-tuple-element.12), kind=kLoop, calls=%fused_computation | loop fusion | flops 1048576 | bytes 5242880 | tf_op jit(solution)/shard_map/add | solution.py:840
  143.8 0.0 copy-done.1
  143.8 0.0 copy-start
  143.8 1.5 %convert_element_type.13 = f32[256,2048]{1,0:T(8,128)} convert(bf16[256,2048]{1,0:T(8,128)(2,1)S(1)} %copy-done.1) | non-fusion elementwise | flops 524288 | bytes 3145728 | tf_op jit(solution)/shard_map/convert_element_type | solution.py:839
  145.3 0.0 copy-done
  145.3 0.0 copy-start.3
  145.3 0.0 copy-start.2
  145.3 1.5 %bitcast_convert_fusion = f32[2048,256]{1,0:T(8,128)} fusion(bf16[4,4,128,256]{3,2,1,0:T(8,128)(2,1)S(1)} %copy-done), kind=kLoop, calls=%fused_computation.1 | loop fusion | flops 524288 | bytes 3145728 | tf_op jit(solution)/shard_map/convert_element_type | solution.py:841
  146.9 0.0 copy-done.3
  146.9 0.6 copy.11
  147.5 0.0 copy-done.2
  147.5 0.6 copy.12
Async XLA Ops:
  140.1 3.6 %copy-start.1 = (bf16[256,2048]{1,0:T(8,128)(2,1)S(1)}, bf16[256,2048]{1,0:T(8,128)(2,1)}, u32[]{:S(2)}) copy-start(bf16[256,2048]{1,0:T(8,128)(2,1)} %get-tuple-element.13) | copy-start | bytes 3145732
  143.8 1.6 %copy-start = (bf16[4,4,128,256]{3,2,1,0:T(8,128)(2,1)S(1)}, bf16[4,4,128,256]{3,2,1,0:T(8,128)(2,1)}, u32[]{:S(2)}) copy-start(bf16[4,4,128,256]{3,2,1,0:T(8,128)(2,1)} %get-tuple-element.14) | copy-start | bytes 3145732
  145.3 1.6 %copy-start.3 = (f32[1,256]{1,0:T(1,128)S(1)}, f32[1,256]{1,0:T(1,128)}, u32[]{:S(2)}) copy-start(f32[1,256]{1,0:T(1,128)} %get-tuple-element.15) | copy-start | bytes 3076
  145.3 2.1 %copy-start.2 = (f32[1,2048]{1,0:T(1,128)S(1)}, f32[1,2048]{1,0:T(1,128)}, u32[]{:S(2)}) copy-start(f32[1,2048]{1,0:T(1,128)} %get-tuple-element.16) | copy-start | bytes 24580

commit v7 on v6

--- a/solution.py
+++ b/solution.py
@@ -245,7 +245,7 @@
     tokens_hbm, cot_hbm, up_hbm, down_hbm,
     share_out, extra_out, up_out, down_out, up_norms, down_norms,
     acts, ups, downs, other_up, rectified, pre_grad, other_pre, turned,
-    leaving, inbox, partial, spread, spread_far, share_leaving, share_got, share_sum,
+    leaving, inbox, partial, spread, spread_far, share_leaving, share_got, share_sum, share_all,
     row_norms, col_norms, up_turned,
     send_sems, got_sems, local_sems,
 ):
@@ -602,31 +602,31 @@
         arrived(col_norms.at[1], "core_norms").wait_recv()
         up_norms[...] = col_norms[0, 0:1, :] + col_norms[1, 0:1, :]
 
-    def share_term(owner):
-        at = pl.ds(pl.multiple_of(owner * rows, rows), rows)
-        parts = []
+    def share_add(k):
+        arrived(other_pre.at[k], "core_pre", k).wait_recv()
         for i in range(near):
             line = core * near + i
-            total = None
-            for k in range(splits):
-                for grads, weights in ((pre_grad, ups), (other_pre, other_up)):
-                    a = dot(grads[k, at, :], weights[k, line], 1, 1)
-                    total = a if total is None else total + a
-            parts.append(total)
-        return parts
-
-    def share_send():
-        for k in range(splits):
-            arrived(other_pre.at[k], "core_pre", k).wait_recv()
+            arrived(other_up.at[k, line], "core_up", k, line).wait_recv()
+
+        def body(owner, carry):
+            at = pl.ds(pl.multiple_of(owner * rows, rows), rows)
             for i in range(near):
                 line = core * near + i
-                arrived(other_up.at[k, line], "core_up", k, line).wait_recv()
+                cols = slice(i * wide, (i + 1) * wide)
+                total = dot(pre_grad[k, at, :], ups[k, line], 1, 1)
+                total += dot(other_pre[k, at, :], other_up[k, line], 1, 1)
+                share_all[at, cols] = total if k == 0 else share_all[at, cols] + total
+            return carry
+
+        lax.fori_loop(0, 4, body, 0)
+
+    def share_send():
+        share_add(splits - 1)
         for j, (owner, to) in enumerate(((at_far, to_far), (at_x, to_x), (at_y, to_y))):
-            for i, part in enumerate(share_term(owner)):
-                share_leaving[j, :, i * wide : (i + 1) * wide] = part.astype(jnp.bfloat16)
+            at = pl.ds(pl.multiple_of(owner * rows, rows), rows)
+            share_leaving[j] = share_all[at, :].astype(jnp.bfloat16)
             send(share_leaving.at[j], share_got.at[j], to, "share", j)
-        for i, part in enumerate(share_term(me)):
-            share_sum[:, i * wide : (i + 1) * wide] = part
+        share_sum[...] = share_all[pl.ds(pl.multiple_of(me * rows, rows), rows), :]
 
     share_keys = ("core_share", "core_extra")
 
@@ -730,6 +730,7 @@
         if k + 1 < splits:
             for d in range(1, lines - 1):
                 gather_step(k + 1, d, middle)
+        share_add(k - 1)
         for d in range(1, lines):
             gather_step(k, d, end)
         every(compute, k)
@@ -824,6 +825,7 @@
             pltpu.VMEM((3, rows, width // 2), narrow),
             pltpu.VMEM((3, rows, width // 2), narrow),
             pltpu.VMEM((rows, width // 2), full),
+            pltpu.VMEM((plane, width // 2), full),
             pltpu.VMEM((lines, 4, 1, units // 4), full),
             pltpu.VMEM((2, 8, depth), full),
             pltpu.VMEM((depth, units), narrow),

time: 148 us -> 153 us (1.034); the launches traced: 148 us -> 151 us
  Pallas kernels: 140 us -> 143 us
    pallas_call x1, Pallas kernels: 140 us -> 143 us  [plane_plan(): pl.pallas_call(functools.partial(plane_kernel, lines, splits, sent, got,...]
where the time goes in v7:
time: 153 us; the launch traced here: 151 us
  Pallas kernels  143 us (93%)
  other arithmetic  6.73 us (4%)
    pallas_call x1, Pallas kernels, plane_plan(): pl.pallas_call(functools.partial(plane_kernel, lines, splits, sent, got,...  143 us
    add x1, other arithmetic, plane_plan(): share = share + extra.astype(full)  3.63 us

profile of v7, /device:TPU:0, one launch (start us, length us, event | category | flops | bytes accessed | tf_op | source)
XLA Modules:
  0.0 151.3 jit_solution(10420327876851179456)
XLA Ops:
  0.6 142.8 %plane.1 = (f32[256,2048]{1,0:T(8,128)}, bf16[256,2048]{1,0:T(8,128)(2,1)}, bf16[256,2048]{1,0:T(8,128)(2,1)}, bf16[4,4,128,256]{3,2,1,0:T(8,128)(2,1)}, f32[1,256]{1,0:T(1,128)}, /*index=5*/f32[1,2048]{1,0:T(1,128)}) custom-call(bf16[256,2048]{1,0:T(8,128)(2,1)} %tokens_hbm.1, bf16[256,2048]{1,0:T(8,128)(2,1)} %cot_hbm.1, bf16[256,2048]{1,0:T(8,128)(2,1)} %up_hbm.1, ...), custom_call_target="tpu_custom_call" | custom-call | tf_op jit(solution)/shard_map/plane/pallas_call | solution.py:799
  143.4 0.0 copy-start.1
  143.4 3.6 %convert_add_fusion = f32[256,2048]{1,0:T(8,128)} fusion(f32[256,2048]{1,0:T(8,128)} %get-tuple-element.11, bf16[256,2048]{1,0:T(8,128)(2,1)} %get-tuple-element.12), kind=kLoop, calls=%fused_computation | loop fusion | flops 1048576 | bytes 5242880 | tf_op jit(solution)/shard_map/add | solution.py:842
  147.1 0.0 copy-done.1
  147.1 0.0 copy-start
  147.1 1.5 %convert_element_type.13 = f32[256,2048]{1,0:T(8,128)} convert(bf16[256,2048]{1,0:T(8,128)(2,1)S(1)} %copy-done.1) | non-fusion elementwise | flops 524288 | bytes 3145728 | tf_op jit(solution)/shard_map/convert_element_type | solution.py:841
  148.6 0.0 copy-done
  148.6 0.0 copy-start.3
  148.6 0.0 copy-start.2
  148.6 1.5 %bitcast_convert_fusion = f32[2048,256]{1,0:T(8,128)} fusion(bf16[4,4,128,256]{3,2,1,0:T(8,128)(2,1)S(1)} %copy-done), kind=kLoop, calls=%fused_computation.1 | loop fusion | flops 524288 | bytes 3145728 | tf_op jit(solution)/shard_map/convert_element_type | solution.py:843
  150.2 0.0 copy-done.3
  150.2 0.6 copy.11
  150.7 0.0 copy-done.2
  150.7 0.6 copy.12
Async XLA Ops:
  143.4 3.6 %copy-start.1 = (bf16[256,2048]{1,0:T(8,128)(2,1)S(1)}, bf16[256,2048]{1,0:T(8,128)(2,1)}, u32[]{:S(2)}) copy-start(bf16[256,2048]{1,0:T(8,128)(2,1)} %get-tuple-element.13) | copy-start | bytes 3145732
  147.1 1.6 %copy-start = (bf16[4,4,128,256]{3,2,1,0:T(8,128)(2,1)S(1)}, bf16[4,4,128,256]{3,2,1,0:T(8,128)(2,1)}, u32[]{:S(2)}) copy-start(bf16[4,4,128,256]{3,2,1,0:T(8,128)(2,1)} %get-tuple-element.14) | copy-start | bytes 3145732
  148.6 1.6 %copy-start.3 = (f32[1,256]{1,0:T(1,128)S(1)}, f32[1,256]{1,0:T(1,128)}, u32[]{:S(2)}) copy-start(f32[1,256]{1,0:T(1,128)} %get-tuple-element.15) | copy-start | bytes 3076
  148.6 2.1 %copy-start.2 = (f32[1,2048]{1,0:T(1,128)S(1)}, f32[1,2048]{1,0:T(1,128)}, u32[]{:S(2)}) copy-start(f32[1,2048]{1,0:T(1,128)} %get-tuple-element.16) | copy-start | bytes 24580
